TPU v7x, 256 devices: a whole 4x4x8 slice. The times are simulated.
256 devices in a mesh: ep: 128 (over z, y, x), tp: 2 (over core).
Axes of the slice: x: 4, y: 4, z: 8, core: 2. Of those that a mesh axis runs over, the one named last changes fastest.
Arguments:
- tokens: bfloat16 [2048, 1536], P('ep'), may hold values from -6 to 6
- prior_state: float32 [2048, 12, 64, 64], P('ep', 'tp'), may hold values from -12 to 12
- first_gain: float32 [1536], replicated, may hold values from 0.1 to 1.9
- query_weight: bfloat16 [1536, 768], P(None, 'tp'), may hold values from -0.15625 to 0.15625
- key_weight: bfloat16 [1536, 768], P(None, 'tp'), may hold values from -0.15625 to 0.15625
- value_weight: bfloat16 [1536, 768], P(None, 'tp'), may hold values from -0.15625 to 0.15625
- decay_down: bfloat16 [1536, 96], replicated, may hold values from -0.15625 to 0.15625
- decay_up: bfloat16 [96, 768], P(None, 'tp'), may hold values from -1.25 to 1.25
- decay_base: float32 [768], P('tp'), may hold values from -5 to 1
- rate_down: bfloat16 [1536, 96], replicated, may hold values from -0.15625 to 0.15625
- rate_up: bfloat16 [96, 768], P(None, 'tp'), may hold values from -1.25 to 1.25
- rate_base: float32 [768], P('tp'), may hold values from -4 to 4
- head_gain: float32 [768], P('tp'), may hold values from 0.1 to 1.9
- out_weight: bfloat16 [768, 1536], P('tp'), may hold values from -0.21875 to 0.21875
- mid_gain: float32 [1536], replicated, may hold values from 0.1 to 1.9
- route_ids: int32 [2048, 6], P('ep'), may hold values from 0 to 127, all different within a row; in each aligned block of 16 rows (0 to 15, 16 to 31, ...) at most 2 rows name the same one
- route_weights: float32 [2048, 6], P('ep'), may hold values from 0.1 to 1
- expert_gate: bfloat16 [128, 1536, 384], P('ep', None, 'tp'), may hold values from -0.15625 to 0.15625
- expert_up: bfloat16 [128, 1536, 384], P('ep', None, 'tp'), may hold values from -0.15625 to 0.15625
- expert_down: bfloat16 [128, 384, 1536], P('ep', 'tp'), may hold values from -0.3125 to 0.3125
- dense_gate: bfloat16 [1536, 6144], P(None, ('ep', 'tp')), may hold values from -0.15625 to 0.15625
- dense_up: bfloat16 [1536, 6144], P(None, ('ep', 'tp')), may hold values from -0.15625 to 0.15625
- dense_down: bfloat16 [6144, 1536], P(('ep', 'tp')), may hold values from -0.078125 to 0.078125
- blend_vector: bfloat16 [1536], replicated, may hold values from -0.15625 to 0.15625
Outputs:
- mixed: bfloat16 [2048, 1536], P('ep', 'tp')
- new_state: float32 [2048, 12, 64, 64], P('ep', 'tp')
Inputs may be any that keep to these rules, and one draw needn't show every extreme that they name: `route_ids`: each row names 6 different experts; among the rows of one device no expert is named by more than 2 rows, a bound that some block reaches.
All inputs are finite; a program needn't handle non-finite values.
Results may differ from a plain program's by a relative error of at most 0.02.
Values may be sent and summed in bfloat16 or wider, within the bound.
A program may use at most 128 MiB of HBM per device.

v0:
```python
import jax
import jax.numpy as jnp
from jax import lax
from jax.sharding import Mesh
from jax.sharding import PartitionSpec as P

EP = ("ep_0", "ep_1", "ep_2")
EP_TP = ("ep_0", "ep_1", "ep_2", "tp")


def cut_along(value, dim, length):
    shape = value.shape
    blocks = value.reshape(*shape[:dim], length, shape[dim] // length, *shape[dim + 1 :])
    return jnp.moveaxis(blocks, dim, 0)


def summed_on_arrival(value, axis, dim):
    length = lax.axis_size(axis)
    blocks = lax.all_to_all(cut_along(value, dim, length), axis, 0, 0, tiled=True)
    return jnp.sum(blocks.astype(jnp.float32), axis=0)


def items_in_groups(value, axis, split_dim, concat_dim, work, item_dim, out_dim):

    def moved(group):
        return lax.all_to_all(group, axis, split_axis=split_dim, concat_axis=concat_dim, tiled=True)

    items = jax.tree.leaves(value)[0].shape[item_dim]
    ends = [items * k // 2 for k in range(2 + 1)] if items % 2 == 0 else [0, items]
    groups = [
        jax.tree.map(lambda a: lax.slice_in_dim(a, low, high, axis=item_dim), value)
        for low, high in zip(ends, ends[1:])
    ]
    arrived = [moved(group) for group in groups]
    made = [work(group) for group in arrived]
    return jax.tree.map(lambda *parts: jnp.concatenate(parts, axis=out_dim), *made)


def whole_of(value, axes, dim):
    for axis in reversed(axes):
        value = lax.all_gather(value, axis, axis=dim, tiled=True)
    return value


def rms_norm(values, gain):
    scale = lax.rsqrt(jnp.mean(values * values, axis=-1, keepdims=True) + 1e-06)
    return values * scale * gain


def rounded(values):
    return lax.optimization_barrier(values.astype(jnp.bfloat16)).astype(jnp.float32)


def mixer_core(
    normed,
    prior_state,
    query_weight,
    key_weight,
    value_weight,
    decay_down,
    decay_up,
    decay_base,
    rate_down,
    rate_up,
    rate_base,
    head_gain,
):
    rows = normed.shape[0]
    heads_here = prior_state.shape[1]
    head_size = prior_state.shape[2]

    def project(weight):
        product = jnp.dot(normed, weight, preferred_element_type=jnp.float32)
        return rounded(product).reshape(rows, heads_here, head_size)

    receptance = project(query_weight)
    key_vec = project(key_weight)
    value_vec = project(value_weight)
    decay_low = jnp.tanh(jnp.dot(normed, decay_down, preferred_element_type=jnp.float32)).astype(
        jnp.bfloat16
    )
    decay_log = decay_base + jnp.dot(decay_low, decay_up, preferred_element_type=jnp.float32)
    decay_log = -jax.nn.softplus(-decay_log) - 0.5
    decay_rate = jnp.exp(-jnp.exp(decay_log)).reshape(rows, heads_here, head_size)
    rate_low = jnp.dot(normed, rate_down, preferred_element_type=jnp.float32).astype(jnp.bfloat16)
    learn_rate = jax.nn.sigmoid(
        rate_base + jnp.dot(rate_low, rate_up, preferred_element_type=jnp.float32)
    )
    learn_rate = learn_rate.reshape(rows, heads_here, head_size)
    unit_key = key_vec * lax.rsqrt(jnp.sum(key_vec * key_vec, axis=-1, keepdims=True) + 1e-06)
    removed = jnp.sum(prior_state * unit_key[:, :, None, :], axis=-1)
    new_state = (
        prior_state * decay_rate[:, :, None, :]
        - removed[..., None] * (unit_key * learn_rate)[:, :, None, :]
        + value_vec[..., None] * key_vec[:, :, None, :]
    )
    read = jnp.sum(new_state * receptance[:, :, None, :], axis=-1)
    center = jnp.mean(read, axis=-1, keepdims=True)
    spread = jnp.mean(jnp.square(read - center), axis=-1, keepdims=True)
    normal = (read - center) * lax.rsqrt(spread + 0.00064)
    mixed_heads = (normal.reshape(rows, -1) * head_gain).astype(jnp.bfloat16)
    return (mixed_heads, new_state)


def shards(
    tokens,
    prior_state,
    first_gain,
    query_weight,
    key_weight,
    value_weight,
    decay_down,
    decay_up,
    decay_base,
    rate_down,
    rate_up,
    rate_base,
    head_gain,
    out_weight,
    mid_gain,
    route_ids,
    route_weights,
    expert_gate,
    expert_up,
    expert_down,
    dense_gate,
    dense_up,
    dense_down,
    blend_vector,
):
    count_ep = lax.axis_size(EP)
    count_tp = lax.axis_size("tp")
    seqs = tokens.shape[0]
    width = tokens.shape[1]
    top_count = route_ids.shape[1]
    half_width = width // count_tp
    capacity = max(2, 2 * seqs * top_count // count_ep)
    token_f = tokens.astype(jnp.float32)
    normed = rms_norm(token_f, first_gain).astype(jnp.bfloat16)
    mixed_heads, new_state = mixer_core(
        normed,
        prior_state,
        query_weight,
        key_weight,
        value_weight,
        decay_down,
        decay_up,
        decay_base,
        rate_down,
        rate_up,
        rate_base,
        head_gain,
    )
    partial_value = jnp.dot(mixed_heads, out_weight, preferred_element_type=jnp.float32)
    attn = lax.psum(partial_value.astype(jnp.bfloat16), "tp").astype(jnp.float32)
    resid = rounded(token_f + attn)
    mid = rms_norm(resid, mid_gain).astype(jnp.bfloat16)
    blend = jax.nn.sigmoid(jnp.dot(mid, blend_vector, preferred_element_type=jnp.float32))
    flat_ids = route_ids.reshape(-1)
    onehot = (flat_ids[:, None] == jnp.arange(count_ep, dtype=jnp.int32)[None, :]).astype(jnp.int32)
    before = jnp.cumsum(onehot, axis=0) - onehot
    position = jnp.sum(onehot * before, axis=1)
    slot = flat_ids * capacity + position
    send = (
        jnp.zeros((count_ep * capacity, width), jnp.bfloat16)
        .at[slot]
        .set(jnp.repeat(mid, top_count, axis=0))
    )
    send = send.reshape(count_ep, capacity, width)
    gate_w = expert_gate[0]
    up_w = expert_up[0]
    down_w = expert_down[0]

    def run_expert(arrived):
        senders = arrived.shape[0]
        items = arrived.shape[1]
        rows_in = arrived.reshape(-1, width)
        hidden = (
            jax.nn.silu(jnp.dot(rows_in, gate_w, preferred_element_type=jnp.float32))
            * jnp.dot(rows_in, up_w, preferred_element_type=jnp.float32)
        ).astype(jnp.bfloat16)
        partial_out = jnp.dot(hidden, down_w, preferred_element_type=jnp.float32)
        summed = summed_on_arrival(partial_out.astype(jnp.bfloat16), "tp", 1)
        result = summed.astype(jnp.bfloat16).reshape(senders, items, half_width)
        return lax.all_to_all(result, EP, split_axis=0, concat_axis=0, tiled=True)

    back = items_in_groups(send, EP, 0, 0, run_expert, 1, 1)
    picked = (
        back.reshape(-1, half_width)[slot].astype(jnp.float32).reshape(seqs, top_count, half_width)
    )
    share = route_weights / jnp.sum(route_weights, axis=1, keepdims=True) * 2.5
    routed = jnp.sum(share[..., None] * picked, axis=1)
    piece = whole_of(mid, EP, 0)
    hidden_all = (
        jax.nn.silu(jnp.dot(piece, dense_gate, preferred_element_type=jnp.float32))
        * jnp.dot(piece, dense_up, preferred_element_type=jnp.float32)
    ).astype(jnp.bfloat16)
    own_units = lax.all_to_all(hidden_all, EP, split_axis=0, concat_axis=1, tiled=True)
    unit_sums = jnp.dot(own_units, whole_of(dense_down, EP, 0), preferred_element_type=jnp.float32)
    dense_out = summed_on_arrival(unit_sums.astype(jnp.bfloat16), "tp", 1)
    own_cols = lax.dynamic_slice_in_dim(resid, lax.axis_index("tp") * half_width, half_width, 1)
    mixed = (own_cols + routed + blend[:, None] * dense_out).astype(jnp.bfloat16)
    return (mixed, new_state)


def solution(mesh):
    split = Mesh(mesh.devices.reshape(8, 4, 4, mesh.shape["tp"]), ("ep_0", "ep_1", "ep_2", "tp"))
    in_specs = (
        P(EP, None),
        P(EP, "tp", None, None),
        P(),
        P(None, "tp"),
        P(None, "tp"),
        P(None, "tp"),
        P(),
        P(None, "tp"),
        P("tp"),
        P(),
        P(None, "tp"),
        P("tp"),
        P("tp"),
        P("tp", None),
        P(),
        P(EP, None),
        P(EP, None),
        P(EP, None, "tp"),
        P(EP, None, "tp"),
        P(EP, "tp", None),
        P(None, EP_TP),
        P(None, EP_TP),
        P(EP_TP, None),
        P(),
    )
    out_specs = (P(EP, "tp"), P(EP, "tp", None, None))
    return jax.shard_map(
        shards, mesh=split, in_specs=in_specs, out_specs=out_specs, check_vma=False
    )
```

profile of v0, /device:TPU:1, one launch (start us, length us, event | category | flops | bytes accessed | tf_op | source)
XLA Modules:
  0.0 297.1 jit_solution(13317201303683752603)
XLA Ops:
  7.3 12.7 %all_gather.21 = bf16[96,1536]{1,0:T(8,128)(2,1)} all-gather(bf16[24,1536]{1,0:T(8,128)(2,1)} %param.46), channel_id=1, replica_groups=mesh['ep_0'=8,'ep_1'=4,'ep_2'=4,'tp'=2] {'ep_2'}, dimensions={0}, use_global_device_ids=true | all-gather | bytes 368640 | tf_op jit(solution)/shard_map/all_gather | solution.py:41
  20.1 0.9 fusion.42
  21.0 1.6 convolution_convert_fusion.4
  22.7 1.6 convolution_convert_fusion.6
  24.5 0.3 convolution_convert_fusion.5
  24.9 0.4 fusion.11
  25.6 0.4 fusion.63
  26.2 15.7 %multiply_reduce_fusion.1 = (f32[16,6]{1,0:T(8,128)S(1)}, f32[16,6,64]{2,1,0:T(8,128)S(1)}, f32[16,6,64,64]{3,2,1,0:T(8,128)}) fusion(f32[16,6,64]{2,1,0:T(8,128)S(1)} %reshape.162, f32[16,6,64]{2,1,0:T(8,128)S(1)} %reshape.160, f32[16,6,64]{2,1,0:T(8,128)S(1)} %reshape.161, f32[16,6,64]{2,1,0:T(8,128)S(1)} %get-tuple-element.4, ...), kind=kOutput, calls=%fused_computation.6 | output fusion | flops 3538911 | bytes 3318144 | tf_op jit(solution)/shard_map/mul | solution.py:94
  41.9 0.2 multiply_reduce_fusion.5
  42.3 0.3 convolution_convert_fusion.3
  42.6 7.6 %psum.7 = bf16[16,1536]{1,0:T(8,128)(2,1)S(1)} all-reduce(bf16[16,1536]{1,0:T(8,128)(2,1)S(1)} %convolution_convert_fusion.3), channel_id=1, replica_groups=mesh['ep_0'=8,'ep_1'=4,'ep_2'=4,'tp'=2] {'tp'}, use_global_device_ids=true, to_apply=%region_6.7 | all-reduce | flops 24576 | bytes 98304 | tf_op jit(solution)/shard_map/psum | solution.py:155
  50.3 0.5 copy-done.6
  50.9 9.2 %all_gather.18 = bf16[64,1536]{1,0:T(8,128)(2,1)S(1)} all-gather(bf16[16,1536]{1,0:T(8,128)(2,1)S(1)} %multiply_convert_fusion), channel_id=1, replica_groups=mesh['ep_0'=8,'ep_1'=4,'ep_2'=4,'tp'=2] {'ep_2'}, dimensions={0}, use_global_device_ids=true | all-gather | bytes 245760 | tf_op jit(solution)/shard_map/all_gather | solution.py:41
  60.1 11.2 %all_gather.19 = bf16[256,1536]{1,0:T(8,128)(2,1)} all-gather(bf16[64,1536]{1,0:T(8,128)(2,1)S(1)} %all_gather.18), channel_id=1, replica_groups=mesh['ep_0'=8,'ep_1'=4,'ep_2'=4,'tp'=2] {'ep_1'}, dimensions={0}, use_global_device_ids=true | all-gather | bytes 983040 | tf_op jit(solution)/shard_map/all_gather | solution.py:41
  71.4 0.7 all-gather.8.cloned.1.call-update
  72.8 0.2 select_reduce_fusion
  73.0 1.3 scatter_custom_fusion
  74.3 0.3 reshape.150
  74.6 1.1 fusion.76
  75.7 0.5 broadcast.142
  76.2 3.8 %reduce.3 = bf16[128,1536]{1,0:T(8,128)(2,1)} reduce(bf16[128,1,1536]{2,1,0:T(2,128)(2,1)S(1)} %get-tuple-element.7, bf16[]{:T(256)} %broadcast.142), dimensions={1}, to_apply=%get-tuple-element.7.reduce_sub_computation | reduce | bytes 786434 | tf_op jit(solution)/shard_map/slice | solution.py:31
  80.0 1.9 reshape.186
  81.9 15.3 %all-to-all-start.3 = ((bf16[128,2,768]{2,1,0:T(2,128)(2,1)}), bf16[128,2,768]{2,1,0:T(2,128)(2,1)}, u32[]{:S(2)}, u32[]{:S(2)}) async-start(bf16[128,2,768]{2,1,0:T(2,128)(2,1)} %reshape.186), calls=%async_computation.3 | async-start | bytes 786432 | tf_op jit(solution)/shard_map/all_to_all | solution.py:26
  97.2 3.8 %reduce.5 = bf16[128,1536]{1,0:T(8,128)(2,1)} reduce(bf16[128,1,1536]{2,1,0:T(2,128)(2,1)S(1)} %get-tuple-element.6, bf16[]{:T(256)} %broadcast.142), dimensions={1}, to_apply=%get-tuple-element.6.reduce_sub_computation | reduce | bytes 786434 | tf_op jit(solution)/shard_map/slice | solution.py:31
  100.9 1.8 reshape.190
  102.8 13.7 %all-to-all-done.3 = bf16[128,2,768]{2,1,0:T(2,128)(2,1)} async-done(((bf16[128,2,768]{2,1,0:T(2,128)(2,1)}), bf16[128,2,768]{2,1,0:T(2,128)(2,1)}, u32[]{:S(2)}, u32[]{:S(2)}) %all-to-all-start.3) | async-done | bytes 393248 | tf_op jit(solution)/shard_map/all_to_all | solution.py:26
  116.5 2.7 reshape.187
  119.2 0.3 fusion.24
  119.5 2.6 convolution_convert_fusion
  122.2 1.0 copy.76
  123.2 9.4 %all_to_all.54 = bf16[2,128,768]{2,1,0:T(8,128)(2,1)S(1)} all-to-all(bf16[2,128,768]{2,1,0:T(8,128)(2,1)S(1)} %bitcast.88), channel_id=1, replica_groups=mesh['ep_0'=8,'ep_1'=4,'ep_2'=4,'tp'=2] {'tp'}, dimensions={0} | all-to-all | bytes 786432 | tf_op jit(solution)/shard_map/all_to_all | solution.py:19
  132.6 7.2 %all-to-all-start = ((bf16[128,2,768]{2,1,0:T(2,128)(2,1)}), bf16[128,2,768]{2,1,0:T(2,128)(2,1)}, u32[]{:S(2)}, u32[]{:S(2)}) async-start(bf16[128,2,768]{2,1,0:T(2,128)(2,1)} %reshape.190), calls=%async_computation | async-start | bytes 786432 | tf_op jit(solution)/shard_map/all_to_all | solution.py:26
  139.9 0.7 reduce.4
  140.6 0.7 reshape.188
  141.3 19.9 %all-to-all-done = bf16[128,2,768]{2,1,0:T(2,128)(2,1)} async-done(((bf16[128,2,768]{2,1,0:T(2,128)(2,1)}), bf16[128,2,768]{2,1,0:T(2,128)(2,1)}, u32[]{:S(2)}, u32[]{:S(2)}) %all-to-all-start) | async-done | bytes 393248 | tf_op jit(solution)/shard_map/all_to_all | solution.py:26
  161.2 2.7 reshape.191
  164.0 0.3 fusion.26
  164.3 1.9 convolution_convert_fusion.1
  166.2 5.2 %all_to_all.55 = bf16[2,128,768]{2,1,0:T(8,128)(2,1)S(1)} all-to-all(bf16[2,128,768]{2,1,0:T(8,128)(2,1)S(1)} %bitcast.89), channel_id=1, replica_groups=mesh['ep_0'=8,'ep_1'=4,'ep_2'=4,'tp'=2] {'tp'}, dimensions={0} | all-to-all | bytes 786432 | tf_op jit(solution)/shard_map/all_to_all | solution.py:19
  171.5 6.2 %all-to-all-start.5 = ((bf16[128,2,384]{2,1,0:T(2,128)(2,1)}), bf16[128,2,384]{2,1,0:T(2,128)(2,1)S(1)}, u32[]{:S(2)}, u32[]{:S(2)}) async-start(bf16[128,2,384]{2,1,0:T(2,128)(2,1)} %reshape.188), calls=%async_computation.5 | async-start | bytes 393216 | tf_op jit(solution)/shard_map/all_to_all | solution.py:185
  177.7 0.7 reduce.6
  178.5 0.7 reshape.192
  179.2 10.9 %all-to-all-done.5 = bf16[128,2,384]{2,1,0:T(2,128)(2,1)S(1)} async-done(((bf16[128,2,384]{2,1,0:T(2,128)(2,1)}), bf16[128,2,384]{2,1,0:T(2,128)(2,1)S(1)}, u32[]{:S(2)}, u32[]{:S(2)}) %all-to-all-start.5) | async-done | bytes 196640 | tf_op jit(solution)/shard_map/all_to_all | solution.py:185
  190.1 6.5 %all-to-all-start.2 = ((bf16[128,2,384]{2,1,0:T(2,128)(2,1)}), bf16[128,2,384]{2,1,0:T(2,128)(2,1)S(1)}, u32[]{:S(2)}, u32[]{:S(2)}) async-start(bf16[128,2,384]{2,1,0:T(2,128)(2,1)} %reshape.192), calls=%async_computation.2 | async-start | bytes 393216 | tf_op jit(solution)/shard_map/all_to_all | solution.py:185
  196.8 0.2 reshape.189
  197.0 14.3 %all-to-all-done.2 = bf16[128,2,384]{2,1,0:T(2,128)(2,1)S(1)} async-done(((bf16[128,2,384]{2,1,0:T(2,128)(2,1)}), bf16[128,2,384]{2,1,0:T(2,128)(2,1)S(1)}, u32[]{:S(2)}, u32[]{:S(2)}) %all-to-all-start.2) | async-done | bytes 196640 | tf_op jit(solution)/shard_map/all_to_all | solution.py:185
  211.3 0.1 reshape.193
  211.5 4.8 %fusion.77 = f32[2048,24]{0,1:T(8,128)S(1)} fusion(bf16[2048,1536]{1,0:T(8,128)(2,1)} %all-gather.4.cloned.1.call-done, bf16[1536,24]{0,1:T(8,128)(2,1)S(1)} %copy-done.13), kind=kOutput, calls=%fused_computation.113 | convolution fusion | flops 150994944 | bytes 6561792 | tf_op jit(solution)/shard_map/dot_general | solution.py:195
  216.3 1.7 fusion.2
  218.0 0.3 copy.49
  218.3 1.2 reshape.184
  219.5 6.2 %all-to-all-start.6 = ((bf16[128,2,192]{2,1,0:T(2,128)(2,1)}), bf16[128,2,192]{2,1,0:T(2,128)(2,1)S(1)}, u32[]{:S(2)}, u32[]{:S(2)}) async-start(bf16[128,2,192]{2,1,0:T(2,128)(2,1)} %reshape.184), calls=%async_computation.6 | async-start | bytes 262144 | tf_op jit(solution)/shard_map/all_to_all | solution.py:198
  225.7 0.9 pad_maximum_fusion
  226.6 0.1 reshape.157
  226.7 0.8 gather_fusion
  227.6 0.2 multiply_reduce_fusion.3
  227.8 10.7 %all-to-all-done.6 = bf16[128,2,192]{2,1,0:T(2,128)(2,1)S(1)} async-done(((bf16[128,2,192]{2,1,0:T(2,128)(2,1)}), bf16[128,2,192]{2,1,0:T(2,128)(2,1)S(1)}, u32[]{:S(2)}, u32[]{:S(2)}) %all-to-all-start.6) | async-done | bytes 98336 | tf_op jit(solution)/shard_map/all_to_all | solution.py:198
  238.4 0.4 reshape.185
  238.9 0.1 copy.47
  239.0 0.7 all_to_all.44
  239.7 41.2 %all-gather.8.cloned.1.call-done = bf16[3072,1536]{1,0:T(8,128)(2,1)} async-done(((bf16[384,1536]{1,0:T(8,128)(2,1)}), bf16[3072,1536]{1,0:T(8,128)(2,1)}) %all-gather.8.cloned.1.call-update) | async-done | bytes 9437200 | tf_op jit(solution)/shard_map/all_gather | solution.py:41
  280.9 5.0 %convolution_convert_fusion.2 = bf16[16,1536]{1,0:T(8,128)(2,1)S(1)} fusion(bf16[16,3072]{1,0:T(8,128)(2,1)S(1)} %all_to_all.44, bf16[3072,1536]{1,0:T(8,128)(2,1)} %all-gather.8.cloned.1.call-done), kind=kOutput, calls=%fused_computation.12 | convolution fusion | flops 151019520 | bytes 9584640 | tf_op jit(solution)/shard_map/dot_general | solution.py:199
  285.9 4.0 %all_to_all.56 = bf16[2,16,768]{2,1,0:T(8,128)(2,1)S(1)} all-to-all(bf16[2,16,768]{2,1,0:T(8,128)(2,1)S(1)} %bitcast.95), channel_id=1, replica_groups=mesh['ep_0'=8,'ep_1'=4,'ep_2'=4,'tp'=2] {'tp'}, dimensions={0} | all-to-all | bytes 98304 | tf_op jit(solution)/shard_map/all_to_all | solution.py:19
  289.9 0.7 add_convert_fusion
  (94 shorter events, 2.6 us)
Async XLA Ops:
  7.2 35.1 %copy-start = (bf16[384,1536]{1,0:T(8,128)(2,1)S(1)}, bf16[384,1536]{1,0:T(8,128)(2,1)}, u32[]{:S(2)}) copy-start(bf16[384,1536]{1,0:T(8,128)(2,1)} %param.37) | copy-start | bytes 3538948
  7.2 17.3 %copy-start.2 = (bf16[16,1536]{1,0:T(8,128)(2,1)S(1)}, bf16[16,1536]{1,0:T(8,128)(2,1)}, u32[]{:S(2)}) copy-start(bf16[16,1536]{1,0:T(8,128)(2,1)} %param.24) | copy-start | bytes 147460
  7.2 17.3 %copy-start.12 = (f32[1536]{0:T(1024)S(1)}, f32[1536]{0:T(1024)}, u32[]{:S(2)}) copy-start(f32[1536]{0:T(1024)} %param.26) | copy-start | bytes 18436
  7.2 17.3 %copy-start.5 = (bf16[1536,384]{1,0:T(8,128)(2,1)S(1)}, bf16[1536,384]{1,0:T(8,128)(2,1)}, u32[]{:S(2)}) copy-start(bf16[1536,384]{1,0:T(8,128)(2,1)} %param.29) | copy-start | bytes 3538948
  7.2 17.7 %copy-start.14 = (bf16[96,384]{1,0:T(8,128)(2,1)S(1)}, bf16[96,384]{1,0:T(8,128)(2,1)}, u32[]{:S(2)}) copy-start(bf16[96,384]{1,0:T(8,128)(2,1)} %param.34) | copy-start | bytes 221188
  7.2 17.7 %copy-start.10 = (bf16[1536,96]{0,1:T(8,128)(2,1)S(1)}, bf16[1536,96]{0,1:T(8,128)(2,1)}, u32[]{:S(2)}) copy-start(bf16[1536,96]{0,1:T(8,128)(2,1)} %param.33) | copy-start | bytes 884740
  7.2 17.7 %copy-start.21 = (f32[384]{0:T(512)S(1)}, f32[384]{0:T(512)}, u32[]{:S(2)}) copy-start(f32[384]{0:T(512)} %param.35) | copy-start | bytes 4612
  7.2 18.3 %copy-start.15 = (bf16[96,384]{1,0:T(8,128)(2,1)S(1)}, bf16[96,384]{1,0:T(8,128)(2,1)}, u32[]{:S(2)}) copy-start(bf16[96,384]{1,0:T(8,128)(2,1)} %param.31) | copy-start | bytes 221188
  7.3 18.3 %copy-start.11 = (bf16[1536,96]{0,1:T(8,128)(2,1)S(1)}, bf16[1536,96]{0,1:T(8,128)(2,1)}, u32[]{:S(2)}) copy-start(bf16[1536,96]{0,1:T(8,128)(2,1)} %param.30) | copy-start | bytes 884740
  7.3 18.3 %copy-start.22 = (f32[384]{0:T(512)S(1)}, f32[384]{0:T(512)}, u32[]{:S(2)}) copy-start(f32[384]{0:T(512)} %param.32) | copy-start | bytes 4612
  7.3 64.1 %all-gather.6.cloned.1.call-start = ((), (), s32[]{:S(2)}) async-start(), calls=%async_computation.9 | async-start | bytes 1474560 | tf_op jit(solution)/shard_map/all_gather | solution.py:41
  20.0 191.4 %all-gather.4.cloned.1.call-start = ((), (), s32[]{:S(2)}) async-start(), calls=%async_computation.8 | async-start | bytes 7077888 | tf_op jit(solution)/shard_map/all_gather | solution.py:41
  26.2 16.1 %copy-start.23 = (f32[384]{0:T(512)S(1)}, f32[384]{0:T(512)}, u32[]{:S(2)}) copy-start(f32[384]{0:T(512)} %param.36) | copy-start | bytes 4612
  26.2 24.6 %copy-start.19 = (f32[1536]{0:T(1024)S(1)}, f32[1536]{0:T(1024)}, u32[]{:S(2)}) copy-start(f32[1536]{0:T(1024)} %param.38) | copy-start | bytes 18436
  41.9 30.1 %copy-start.17 = (s32[16,6]{0,1:T(8,128)S(1)}, s32[16,6]{0,1:T(8,128)}, u32[]{:S(2)}) copy-start(s32[16,6]{0,1:T(8,128)} %param.39) | copy-start | bytes 1156
  50.2 0.6 copy-start.6
  50.9 22.1 %copy-start.8 = (bf16[16,1536]{1,0:T(8,128)(2,1)}, bf16[16,1536]{1,0:T(8,128)(2,1)S(1)}, u32[]{:S(2)}) copy-start(bf16[16,1536]{1,0:T(8,128)(2,1)S(1)} %multiply_convert_fusion) | copy-start | bytes 147460
  71.3 209.6 %all-gather.8.cloned.1.call-start = ((), (), s32[]{:S(2)}) async-start(), calls=%async_computation.10 | async-start | bytes 10616832 | tf_op jit(solution)/shard_map/all_gather | solution.py:41
  75.7 43.5 %copy-start.3 = (bf16[1,1536,192]{1,2,0:T(8,128)(2,1)S(1)}, bf16[1,1536,192]{1,2,0:T(8,128)(2,1)}, u32[]{:S(2)}) copy-start(bf16[1,1536,192]{1,2,0:T(8,128)(2,1)} %param.41) | copy-start | bytes 1769476
  80.0 39.5 %copy-start.4 = (bf16[1,192,1536]{2,1,0:T(8,128)(2,1)S(1)}, bf16[1,192,1536]{2,1,0:T(8,128)(2,1)}, u32[]{:S(2)}) copy-start(bf16[1,192,1536]{2,1,0:T(8,128)(2,1)} %param.43) | copy-start | bytes 1769476
  81.9 34.6 %all-to-all-start.3 = ((bf16[128,2,768]{2,1,0:T(2,128)(2,1)}), bf16[128,2,768]{2,1,0:T(2,128)(2,1)}, u32[]{:S(2)}, u32[]{:S(2)}) async-start(bf16[128,2,768]{2,1,0:T(2,128)(2,1)} %reshape.186), calls=%async_computation.3 | async-start | bytes 786432 | tf_op jit(solution)/shard_map/all_to_all | solution.py:26
  132.6 28.7 %all-to-all-start = ((bf16[128,2,768]{2,1,0:T(2,128)(2,1)}), bf16[128,2,768]{2,1,0:T(2,128)(2,1)}, u32[]{:S(2)}, u32[]{:S(2)}) async-start(bf16[128,2,768]{2,1,0:T(2,128)(2,1)} %reshape.190), calls=%async_computation | async-start | bytes 786432 | tf_op jit(solution)/shard_map/all_to_all | solution.py:26
  141.3 36.3 %copy-start.18 = (f32[16,6]{0,1:T(8,128)S(1)}, f32[16,6]{0,1:T(8,128)}, u32[]{:S(2)}) copy-start(f32[16,6]{0,1:T(8,128)} %param.40) | copy-start | bytes 1156
  164.3 32.3 %copy-start.7 = (bf16[16,1536]{1,0:T(8,128)(2,1)S(1)}, bf16[16,1536]{1,0:T(8,128)(2,1)}, u32[]{:S(2)}) copy-start(bf16[16,1536]{1,0:T(8,128)(2,1)} %copy-done.6) | copy-start | bytes 147460
  164.3 32.4 %copy-start.20 = (bf16[1536]{0:T(1024)(128)(2,1)S(1)}, bf16[1536]{0:T(1024)(128)(2,1)}, u32[]{:S(2)}) copy-start(bf16[1536]{0:T(1024)(128)(2,1)} %param.47) | copy-start | bytes 9220
  164.3 32.4 %copy-start.9 = (bf16[16,1536]{1,0:T(8,128)(2,1)S(1)}, bf16[16,1536]{1,0:T(8,128)(2,1)}, u32[]{:S(2)}) copy-start(bf16[16,1536]{1,0:T(8,128)(2,1)} %copy-done.8) | copy-start | bytes 147460
  164.3 47.1 %copy-start.13 = (bf16[1536,24]{0,1:T(8,128)(2,1)S(1)}, bf16[1536,24]{0,1:T(8,128)(2,1)}, u32[]{:S(2)}) copy-start(bf16[1536,24]{0,1:T(8,128)(2,1)} %param.44) | copy-start | bytes 221188
  171.5 18.6 %all-to-all-start.5 = ((bf16[128,2,384]{2,1,0:T(2,128)(2,1)}), bf16[128,2,384]{2,1,0:T(2,128)(2,1)S(1)}, u32[]{:S(2)}, u32[]{:S(2)}) async-start(bf16[128,2,384]{2,1,0:T(2,128)(2,1)} %reshape.188), calls=%async_computation.5 | async-start | bytes 393216 | tf_op jit(solution)/shard_map/all_to_all | solution.py:185
  190.1 21.2 %all-to-all-start.2 = ((bf16[128,2,384]{2,1,0:T(2,128)(2,1)}), bf16[128,2,384]{2,1,0:T(2,128)(2,1)S(1)}, u32[]{:S(2)}, u32[]{:S(2)}) async-start(bf16[128,2,384]{2,1,0:T(2,128)(2,1)} %reshape.192), calls=%async_computation.2 | async-start | bytes 393216 | tf_op jit(solution)/shard_map/all_to_all | solution.py:185
  211.4 4.8 %copy-start.16 = (bf16[1536,24]{0,1:T(8,128)(2,1)S(1)}, bf16[1536,24]{0,1:T(8,128)(2,1)}, u32[]{:S(2)}) copy-start(bf16[1536,24]{0,1:T(8,128)(2,1)} %param.45) | copy-start | bytes 221188
  211.5 4.8 %copy-start.1 = (bf16[2048,1536]{1,0:T(8,128)(2,1)S(1)}, bf16[2048,1536]{1,0:T(8,128)(2,1)}, u32[]{:S(2)}) copy-start(bf16[2048,1536]{1,0:T(8,128)(2,1)} %all-gather.4.cloned.1.call-done) | copy-start | bytes 18874372
  219.5 18.9 %all-to-all-start.6 = ((bf16[128,2,192]{2,1,0:T(2,128)(2,1)}), bf16[128,2,192]{2,1,0:T(2,128)(2,1)S(1)}, u32[]{:S(2)}, u32[]{:S(2)}) async-start(bf16[128,2,192]{2,1,0:T(2,128)(2,1)} %reshape.184), calls=%async_computation.6 | async-start | bytes 262144 | tf_op jit(solution)/shard_map/all_to_all | solution.py:198
Sparse Core Ops, SparseCore 0:
  20.1 29.0 all-gather.5
  71.4 96.9 all-gather.3
  170.2 110.7 all-gather.7
where the time goes:
time: 298 us; the launch traced here: 297 us
  waiting for transfers between devices  111 us (37%)
  blocking collectives  59.2 us (20%)
  starting transfers between devices  41.4 us (14%)
  other arithmetic  28.7 us (10%)
  matrix products  21.4 us (7%)
  local copies, waits for them, and re-layouts  20.6 us (7%)
  between operations  14.4 us (5%)
    all_gather x3, waiting for transfers between devices, whole_of(): value = lax.all_gather(value, axis, axis=dim, tiled=True)  41.2 us
    all_to_all x2, waiting for transfers between devices, moved(): lax.all_to_all(group, axis, split_axis=split_dim, concat_axis=concat_dim,...  33.6 us
    all_gather x3, blocking collectives, whole_of(): value = lax.all_gather(value, axis, axis=dim, tiled=True)  33 us
    all_to_all x2, waiting for transfers between devices, run_expert(): return lax.all_to_all(result, EP, split_axis=0, concat_axis=0, tiled=True)  25.2 us
    all_to_all x2, starting transfers between devices, moved(): lax.all_to_all(group, axis, split_axis=split_dim, concat_axis=concat_dim,...  22.5 us
    all_to_all x3, blocking collectives, summed_on_arrival(): lax.all_to_all(cut_along(value, dim, length), axis, 0, 0, tiled=True)  18.6 us
    mul x1, other arithmetic, mixer_core(): removed[..., None] * (unit_key * learn_rate)[:, :, None, :]  15.7 us
    unnamed x60, local copies, waits for them, and re-layouts  13.2 us
  transfers between devices with their start and end apart: 8, of which 6 were waited for; matrix products, arithmetic and copies ran while one was open for 21% of the time, Pallas kernels for 0%

commit v1 on v0

v1 whole, which is shorter than its diff:
```python
import functools

import jax
import jax.numpy as jnp
from jax import lax
from jax.experimental import pallas as pl
from jax.experimental.pallas import tpu as pltpu
from jax.sharding import Mesh
from jax.sharding import PartitionSpec as P

EP = ("ep_0", "ep_1", "ep_2")
EP_TP = ("ep_0", "ep_1", "ep_2", "tp")
NZ, NY, NX = 8, 4, 4
F32 = jnp.float32
BF16 = jnp.bfloat16
MESH_ID = pl.DeviceIdType.MESH
VMEM = pltpu.VMEM

D = 1536
ROWS = 8
WIDE = D + 128
AGA = slice(0, 512)
AGB = slice(512, 1024)
AGAB = slice(0, 1024)
AGC = slice(1024, WIDE)
CA = slice(0, 512)
CB = slice(512, 1024)
CC = slice(1024, 1536)
W = 512
N_COPIES = 192


def dot(a, b):
    return jnp.dot(a, b, preferred_element_type=F32)


def mixer_kernel(
    tok, gain, wq_h, wk_h, wv_h, dd, du, db, rd, ru, rb, hg, wo_h, st_h,
    part, st_out,
    wq, wk, wv, wo, st, dec_s, unit_s, ul_s, key_s, rec_s, val_s, mix_s, wsem, isem, osem,
):
    heads = st_h.shape[1]
    rows = tok.shape[0]
    loads = [
        pltpu.make_async_copy(src, dst, wsem.at[i])
        for i, (src, dst) in enumerate(((wk_h, wk), (wv_h, wv), (wq_h, wq), (wo_h, wo)))
    ]
    for load in loads[:3]:
        load.start()
    states = [pltpu.make_async_copy(st_h.at[:, h], st.at[h], isem.at[h]) for h in range(heads)]
    for copy in states:
        copy.start()
    loads[3].start()
    token_f = tok[...].astype(F32)
    scale = lax.rsqrt(jnp.mean(token_f * token_f, axis=-1, keepdims=True) + 1e-06)
    normed = (token_f * scale * gain[...]).astype(BF16)
    decay_low = jnp.tanh(dot(normed, dd[...])).astype(BF16)
    decay_in = db[...] + dot(decay_low, du[...])
    decay = jnp.exp(-0.6065306597126334 * jax.nn.sigmoid(decay_in))
    rate_low = dot(normed, rd[...]).astype(BF16)
    learn = jax.nn.sigmoid(rb[...] + dot(rate_low, ru[...]))
    loads[0].wait()
    key = dot(normed, wk[...]).astype(BF16).astype(F32)
    loads[1].wait()
    value = dot(normed, wv[...]).astype(BF16).astype(F32)
    loads[2].wait()
    rec = dot(normed, wq[...]).astype(BF16).astype(F32)
    value_t = jnp.transpose(value)
    for h in range(heads):
        lanes = slice(64 * h, 64 * h + 64)
        k = key[:, lanes]
        unit = k * lax.rsqrt(jnp.sum(k * k, axis=-1, keepdims=True) + 1e-06)
        key_s[h] = k
        unit_s[h] = unit
        ul_s[h] = unit * learn[:, lanes]
        dec_s[h] = decay[:, lanes]
        rec_s[h] = rec[:, lanes]
        val_s[h] = value_t[64 * h : 64 * h + 64, :]

    lane = lax.broadcasted_iota(jnp.int32, (64, 128), 1)

    def head(h, carry):
        pltpu.make_async_copy(st_h.at[:, h], st.at[h], isem.at[h]).wait()
        reads = jnp.zeros((64, 128), F32)
        for b in range(rows):
            prior = st[h, b]
            removed = jnp.sum(prior * unit_s[h, b : b + 1, :], axis=1, keepdims=True)
            new = (
                prior * dec_s[h, b : b + 1, :]
                - removed * ul_s[h, b : b + 1, :]
                + val_s[h, :, b : b + 1] * key_s[h, b : b + 1, :]
            )
            st[h, b] = new
            read = jnp.sum(new * rec_s[h, b : b + 1, :], axis=1, keepdims=True)
            reads = jnp.where(lane == b, read, reads)
        pltpu.make_async_copy(st.at[h], st_out.at[:, h], osem.at[h]).start()
        center = jnp.mean(reads, axis=0, keepdims=True)
        diff = reads - center
        spread = jnp.mean(diff * diff, axis=0, keepdims=True)
        mix_s[pl.ds(pl.multiple_of(h * 64, 64), 64), :] = diff * lax.rsqrt(spread + 0.00064) * hg[h]
        return carry

    lax.fori_loop(0, heads, head, 0)
    mixed = jnp.transpose(mix_s[...])[0:rows, :].astype(BF16)
    loads[3].wait()
    partial = dot(mixed, wo[...])
    part[0] = partial[0:8].astype(BF16)
    part[1] = partial[8:16].astype(BF16)

    def drain(h, carry):
        pltpu.make_async_copy(st.at[h], st_out.at[:, h], osem.at[h]).wait()
        return carry

    lax.fori_loop(0, heads, drain, 0)


def mixer(tokens, prior_state, first_gain, wq, wk, wv, dd, du, db, rd, ru, rb, hg, wo):
    rows, heads = prior_state.shape[:2]
    vm = pl.BlockSpec(memory_space=VMEM)
    hbm = pl.BlockSpec(memory_space=pl.ANY)
    inner = heads * 64
    small = VMEM((heads, rows, 64), F32)
    return pl.pallas_call(
        mixer_kernel,
        name="mixer",
        out_shape=(
            jax.ShapeDtypeStruct((2, rows // 2, D), BF16),
            jax.ShapeDtypeStruct(prior_state.shape, F32),
        ),
        in_specs=[vm, vm, hbm, hbm, hbm, vm, vm, vm, vm, vm, vm, vm, hbm, hbm],
        out_specs=(vm, hbm),
        scratch_shapes=[
            VMEM((D, inner), BF16), VMEM((D, inner), BF16), VMEM((D, inner), BF16),
            VMEM((inner, D), BF16), VMEM((heads, rows, 64, 64), F32),
            small, small, small, small, small,
            VMEM((heads, 64, rows), F32), VMEM((inner, 128), F32),
            pltpu.SemaphoreType.DMA((4,)),
            pltpu.SemaphoreType.DMA((heads,)),
            pltpu.SemaphoreType.DMA((heads,)),
        ],
    )(
        tokens, first_gain.reshape(1, D), wq, wk, wv, dd, du, db.reshape(1, inner), rd, ru,
        rb.reshape(1, inner), hg.reshape(heads, 64, 1), wo, prior_state,
    )


def exchange_kernel(
    part, tok, gain, ids, weights, blend, eg_h, eu_h, ed_h, dg_h, du_h, dd_h,
    out,
    full, made, w1, w2, eg, eu, dg, du, peer_part, fin, fin_in,
    ax1, axf, ay1, ayf, bx1, bxf, by1, byf, a2, b2, z3, r3, cz, c2, ry, c3, rx,
    send_sem, recv_sem, load_sem,
):
    z, y, x = (lax.axis_index(a) for a in EP)
    c = lax.axis_index("tp")
    expert = (z * NY + y) * NX + x
    count = [0]
    started = []

    def xa(d):
        return lax.rem(x + d + NX, NX)

    def ya(d):
        return lax.rem(y + d + NY, NY)

    def za(d):
        return lax.rem(z + d + NZ, NZ)

    def dev(dx=0, dy=0, dz=0, dc=0):
        return {
            "ep_0": za(dz) if dz else z,
            "ep_1": ya(dy) if dy else y,
            "ep_2": xa(dx) if dx else x,
            "tp": 1 - c if dc else c,
        }

    def send(src, dst, to):
        i = count[0]
        count[0] += 1
        copy = pltpu.make_async_remote_copy(
            src_ref=src, dst_ref=dst, send_sem=send_sem.at[i], recv_sem=recv_sem.at[i],
            device_id=to, device_id_type=MESH_ID,
        )
        copy.start()
        started.append(copy)
        return copy

    def rec(copies):
        for copy in copies:
            copy.wait_recv()

    loads = [
        pltpu.make_async_copy(src, dst, load_sem.at[i])
        for i, (src, dst) in enumerate(
            (
                (eg_h.at[0], eg), (eu_h.at[0], eu), (dg_h, dg), (du_h, du),
                (ed_h.at[0], w2.at[0, pl.ds(0, 192), :]),
                (dd_h, w2.at[0, pl.ds(192, 24), :]),
            )
        )
    ]
    for load in loads:
        load.start()

    peers = (
        [dev(dx=d) for d in range(1, NX)]
        + [dev(dy=d) for d in range(1, NY)]
        + [dev(dz=d) for d in range(1, NZ)]
        + [dev(dc=1)]
    )
    barrier = pltpu.get_barrier_semaphore()
    for peer in peers:
        pl.semaphore_signal(barrier, inc=1, device_id=peer, device_id_type=MESH_ID)
    pl.semaphore_wait(barrier, len(peers))

    swap = send(part.at[1 - c], peer_part, dev(dc=1))

    lane = lax.broadcasted_iota(jnp.int32, (ROWS, 128), 1)
    own_w = weights[c]
    own_ids = ids[c]
    share = own_w / jnp.sum(own_w, axis=1, keepdims=True) * 2.5
    shares = jnp.zeros((ROWS, 128), F32)
    for k in range(own_w.shape[1]):
        shares = shares + jnp.where(own_ids[:, k : k + 1] == lane, share[:, k : k + 1], 0.0)
    full[x, y, z, :, D:WIDE] = shares.astype(BF16)

    swap.wait_recv()
    attn = part[c].astype(F32) + peer_part[...].astype(F32)
    resid = (tok[c].astype(F32) + attn).astype(BF16).astype(F32)
    scale = lax.rsqrt(jnp.mean(resid * resid, axis=-1, keepdims=True) + 1e-06)
    full[x, y, z, :, 0:D] = (resid * scale * gain[...]).astype(BF16)

    def same(ref):
        return ref, ref

    zab = [send(*same(full.at[x, y, z, :, AGAB]), dev(dz=d)) for d in (1, 7, 2, 6, 3, 5, 4)]
    cx = [send(*same(full.at[x, y, z, :, AGC]), dev(dx=d)) for d in (1, 3, 2)]

    lo, hi = pl.ds(0, 256), pl.ds(256, 256)
    col = lax.broadcasted_iota(jnp.int32, (192, 256), 1)
    row = lax.broadcasted_iota(jnp.int32, (192, 256), 0)
    place_e = jnp.where(col == row, 1.0, 0.0).astype(BF16)
    col = lax.broadcasted_iota(jnp.int32, (24, 256), 1)
    row = lax.broadcasted_iota(jnp.int32, (24, 256), 0)
    place_d = jnp.where(col == row + 192, 1.0, 0.0).astype(BF16)
    for load in loads:
        load.wait()
    w2[0, 216:256, :] = jnp.zeros((40, D), BF16)
    w1[0, :, 0:256] = (dot(eg[...], place_e) + dot(dg[...], place_d)).astype(BF16)
    w1[0, :, 256:512] = (dot(eu[...], place_e) + dot(du[...], place_d)).astype(BF16)
    w_in = [send(w1.at[0], w1.at[1], dev(dc=1)), send(w2.at[0], w2.at[1], dev(dc=1))]

    rec(cx)
    cy = [send(*same(full.at[:, y, z, :, AGC]), dev(dy=d)) for d in (1, 3, 2)]
    rec(zab)

    def halves_out(ref_of, plus, minus):
        first = [send(*same(ref_of(0, 0)), plus), send(*same(ref_of(0, 1)), minus)]
        second = [send(*same(ref_of(0, 1)), plus), send(*same(ref_of(0, 0)), minus)]
        return first, second

    def halves_on(ref_of, first, plus, minus):
        first[0].wait_recv()
        a = send(*same(ref_of(-1, 0)), plus)
        first[1].wait_recv()
        b = send(*same(ref_of(1, 1)), minus)
        return [a, b]

    def a_y(d, half):
        return full.at[x, ya(d), pl.ds(4 * half, 4), :, AGA]

    def b_x(d, half):
        return full.at[xa(d), y, pl.ds(4 * half, 4), :, AGB]

    def a_x(d, half):
        return full.at[xa(d), pl.ds(2 * half, 2), :, :, AGA]

    def b_y(d, half):
        return full.at[pl.ds(2 * half, 2), ya(d), :, :, AGB]

    yp, ym, xp, xm = dev(dy=1), dev(dy=-1), dev(dx=1), dev(dx=-1)
    ay_1, ay_2 = halves_out(a_y, yp, ym)
    bx_1, bx_2 = halves_out(b_x, xp, xm)
    rec(cy)

    def c_z(d, q):
        return full.at[q, :, za(d), :, AGC]

    def ring_step(s):
        ups = range(4) if s < 4 else (0, 1)
        downs = range(4) if s < 4 else (2, 3)
        return ups, downs

    zp, zm = dev(dz=1), dev(dz=-1)
    ups = {q: send(*same(c_z(0, q)), zp) for q in range(4)}
    downs = {q: send(*same(c_z(0, q)), zm) for q in (2, 3, 0, 1)}

    def c_on(s, ups, downs):
        new_up, new_down = {}, {}
        for q, r in zip((0, 1, 2, 3), (2, 3, 0, 1)):
            ups[q].wait_recv()
            if s < 4 or q in (0, 1):
                new_up[q] = send(*same(c_z(-(s - 1), q)), zp)
            downs[r].wait_recv()
            if s < 4 or r in (2, 3):
                new_down[r] = send(*same(c_z(s - 1, r)), zm)
        return new_up, new_down

    ay_3 = halves_on(a_y, ay_1, yp, ym)
    bx_3 = halves_on(b_x, bx_1, xp, xm)
    ups, downs = c_on(2, ups, downs)
    rec(ay_2 + ay_3)
    ax_1, ax_2 = halves_out(a_x, xp, xm)
    rec(bx_2 + bx_3)
    by_1, by_2 = halves_out(b_y, yp, ym)
    ups, downs = c_on(3, ups, downs)
    ax_3 = halves_on(a_x, ax_1, xp, xm)
    by_3 = halves_on(b_y, by_1, yp, ym)
    ups, downs = c_on(4, ups, downs)
    rec(ax_2 + by_2 + ax_3 + by_3)
    rec(list(ups.values()) + list(downs.values()))
    rec(w_in)

    lane128 = lax.broadcasted_iota(jnp.int32, (256, 128), 1)
    lane256 = lax.broadcasted_iota(jnp.int32, (256, 256), 1)
    bvec = blend[...]

    def layers(xi):
        rows_in = full[xi].reshape(256, WIDE)
        mid = rows_in[:, 0:D]
        chosen = jnp.sum(
            jnp.where(lane128 == expert, rows_in[:, D:WIDE].astype(F32), 0.0), axis=1, keepdims=True
        )
        gate = lax.dot_general(mid, bvec, (((1,), (1,)), ((), ())), preferred_element_type=F32)
        level = jnp.where(lane256 < 192, chosen, jax.nn.sigmoid(gate[:, 0:1]))
        total = None
        for half in range(2):
            both = dot(mid, w1[half])
            g, u = both[:, 0:256], both[:, 256:512]
            hidden = (g * jax.nn.sigmoid(g) * u * level).astype(BF16)
            term = dot(hidden, w2[half])
            total = term if total is None else total + term
        made[xi] = total.astype(BF16).reshape(NY, NZ, ROWS, D)

    layers(xa(2))
    lower, upper = pl.ds(0, 4), pl.ds(4, 4)
    sx = [
        send(made.at[xa(2), :, lower, :, CA], ax1.at[0], xp),
        send(made.at[xa(2), :, upper, :, CA], ax1.at[1], xm),
    ]
    layers(xa(1))
    sx_free = [send(made.at[xa(1), :, upper, :, CA], axf.at[0, :, upper], xp)]
    layers(xa(-1))
    sx_free += [send(made.at[xa(-1), :, lower, :, CA], axf.at[1, :, lower], xm)]
    layers(x)

    def plus(a, b):
        return (a.astype(F32) + b.astype(F32)).astype(BF16)

    c_up, c_down = {}, {}
    c_up[1] = {q: send(made.at[q, :, za(4), :, CC], cz.at[0, 0, q], zp) for q in (0, 1)}
    c_down[1] = {q: send(made.at[q, :, za(4), :, CC], cz.at[1, 0, q], zm) for q in (2, 3)}
    c_up[2] = {q: send(made.at[q, :, za(3), :, CC], cz.at[0, 1, q], zp) for q in (2, 3)}
    c_down[2] = {q: send(made.at[q, :, za(-3), :, CC], cz.at[1, 1, q], zm) for q in (0, 1)}
    sy = [
        send(made.at[:, ya(2), lower, :, CB], by1.at[0], yp),
        send(made.at[:, ya(2), upper, :, CB], by1.at[1], ym),
    ]
    sy_free = [
        send(made.at[:, ya(1), upper, :, CB], byf.at[0, :, upper], yp),
        send(made.at[:, ya(-1), lower, :, CB], byf.at[1, :, lower], ym),
    ]
    sx[0].wait_recv()
    made[xa(1), :, 0:4, :, CA] = plus(made[xa(1), :, 0:4, :, CA], ax1[0])
    sx_free.append(send(made.at[xa(1), :, lower, :, CA], axf.at[0, :, lower], xp))
    sx[1].wait_recv()
    made[xa(-1), :, 4:8, :, CA] = plus(made[xa(-1), :, 4:8, :, CA], ax1[1])
    sx_free.append(send(made.at[xa(-1), :, upper, :, CA], axf.at[1, :, upper], xm))

    def c_back(s):
        for q, r in zip((0, 1, 2, 3), (2, 3, 0, 1)):
            if s > 2 or q in (0, 1):
                c_up[s - 1][q].wait_recv()
                made[q, :, za(5 - s), :, CC] = plus(made[q, :, za(5 - s), :, CC], cz[0, s - 2, q])
                c_up.setdefault(s, {})[q] = send(
                    made.at[q, :, za(5 - s), :, CC], cz.at[0, s - 1, q], zp
                )
            if s > 2 or r in (2, 3):
                c_down[s - 1][r].wait_recv()
                made[r, :, za(s - 5), :, CC] = plus(made[r, :, za(s - 5), :, CC], cz[1, s - 2, r])
                c_down.setdefault(s, {})[r] = send(
                    made.at[r, :, za(s - 5), :, CC], cz.at[1, s - 1, r], zm
                )

    c_back(2)
    sy[0].wait_recv()
    made[:, ya(1), 0:4, :, CB] = plus(made[:, ya(1), 0:4, :, CB], by1[0])
    sy_free.append(send(made.at[:, ya(1), lower, :, CB], byf.at[0, :, lower], yp))
    sy[1].wait_recv()
    made[:, ya(-1), 4:8, :, CB] = plus(made[:, ya(-1), 4:8, :, CB], by1[1])
    sy_free.append(send(made.at[:, ya(-1), upper, :, CB], byf.at[1, :, upper], ym))
    c_back(3)

    def three(a, b, d):
        return (a.astype(F32) + b.astype(F32) + d.astype(F32)).astype(BF16)

    def small_rs(buf, first, final, at, plus_to, minus_to):
        s = [
            send(buf.at[at(2), lower], first.at[0], plus_to),
            send(buf.at[at(2), upper], first.at[1], minus_to),
        ]
        f = [
            send(buf.at[at(1), upper], final.at[0, upper], plus_to),
            send(buf.at[at(-1), lower], final.at[1, lower], minus_to),
        ]
        return s, f

    def small_on(buf, first, final, at, plus_to, minus_to, s):
        s[0].wait_recv()
        buf[at(1), 0:4] = plus(buf[at(1), 0:4], first[0])
        f = [send(buf.at[at(1), lower], final.at[0, lower], plus_to)]
        s[1].wait_recv()
        buf[at(-1), 4:8] = plus(buf[at(-1), 4:8], first[1])
        f.append(send(buf.at[at(-1), upper], final.at[1, upper], minus_to))
        return f

    rec(sx_free)
    a2[...] = three(made[x, :, :, :, CA], axf[0], axf[1])
    a_s, a_f = small_rs(a2, ay1, ayf, ya, yp, ym)
    c_back(4)
    rec(sy_free)
    b2[...] = three(made[:, y, :, :, CB], byf[0], byf[1])
    b_s, b_f = small_rs(b2, bx1, bxf, xa, xp, xm)
    a_f += small_on(a2, ay1, ayf, ya, yp, ym, a_s)
    b_f += small_on(b2, bx1, bxf, xa, xp, xm, b_s)
    rec(list(c_up[4].values()) + list(c_down[4].values()))
    c2[...] = three(made[:, :, z, :, CC], cz[0, 3], cz[1, 3])
    sc = [send(c2.at[:, ya(d)], ry.at[d - 1], dev(dy=d)) for d in (1, 3, 2)]
    rec(a_f)
    z3[:, :, CA] = three(a2[y], ayf[0], ayf[1])
    rec(b_f)
    z3[:, :, CB] = three(b2[x], bxf[0], bxf[1])
    sz = [send(z3.at[za(d)], r3.at[d - 1], dev(dz=d)) for d in (4, 3, 5, 2, 6, 1, 7)]
    rec(sc)
    c3[...] = (
        c2[:, y].astype(F32) + ry[0].astype(F32) + ry[1].astype(F32) + ry[2].astype(F32)
    ).astype(BF16)
    sc = [send(c3.at[xa(d)], rx.at[d - 1], dev(dx=d)) for d in (1, 3, 2)]
    rec(sc)
    last = c3[x].astype(F32) + rx[0].astype(F32) + rx[1].astype(F32) + rx[2].astype(F32)
    fin[:, CC] = (resid[:, CC] + last).astype(BF16)
    rec(sz)
    early = z3[z].astype(F32)
    for d in range(NZ - 1):
        early = early + r3[d].astype(F32)
    fin[:, 0:1024] = (resid[:, 0:1024] + early).astype(BF16)

    half = D // 2
    other = pl.ds(pl.multiple_of((1 - c) * half, 128), half)
    mine = pl.ds(pl.multiple_of(c * half, 128), half)
    swap = send(fin.at[:, other], fin_in, dev(dc=1))
    out[c] = fin[:, mine]
    swap.wait_recv()
    out[1 - c] = fin_in[...]
    for copy in started:
        copy.wait_send()


def exchange(part, tokens, mid_gain, ids, weights, blend, eg, eu, ed, dg, du, dd):
    vm = pl.BlockSpec(memory_space=VMEM)
    hbm = pl.BlockSpec(memory_space=pl.ANY)
    return pl.pallas_call(
        exchange_kernel,
        name="exchange",
        out_shape=jax.ShapeDtypeStruct((2, ROWS, D // 2), BF16),
        in_specs=[vm] * 6 + [hbm] * 6,
        out_specs=vm,
        scratch_shapes=[
            VMEM((NX, NY, NZ, ROWS, WIDE), BF16),
            VMEM((NX, NY, NZ, ROWS, D), BF16),
            VMEM((2, D, 512), BF16),
            VMEM((2, 256, D), BF16),
            VMEM((D, 192), BF16), VMEM((D, 192), BF16),
            VMEM((D, 24), BF16), VMEM((D, 24), BF16),
            VMEM((ROWS, D), BF16), VMEM((ROWS, D), BF16), VMEM((ROWS, D // 2), BF16),
            VMEM((2, NY, 4, ROWS, W), BF16), VMEM((2, NY, NZ, ROWS, W), BF16),
            VMEM((2, 4, ROWS, W), BF16), VMEM((2, NZ, ROWS, W), BF16),
            VMEM((2, 4, ROWS, W), BF16), VMEM((2, NZ, ROWS, W), BF16),
            VMEM((2, NX, 4, ROWS, W), BF16), VMEM((2, NX, NZ, ROWS, W), BF16),
            VMEM((NY, NZ, ROWS, W), BF16), VMEM((NX, NZ, ROWS, W), BF16),
            VMEM((NZ, ROWS, 2 * W), BF16), VMEM((NZ - 1, ROWS, 2 * W), BF16),
            VMEM((2, 4, NX, NY, ROWS, W), BF16), VMEM((NX, NY, ROWS, W), BF16),
            VMEM((NY - 1, NX, ROWS, W), BF16), VMEM((NX, ROWS, W), BF16),
            VMEM((NX - 1, ROWS, W), BF16),
            pltpu.SemaphoreType.DMA((N_COPIES,)),
            pltpu.SemaphoreType.DMA((N_COPIES,)),
            pltpu.SemaphoreType.DMA((6,)),
        ],
        compiler_params=pltpu.CompilerParams(collective_id=0, has_side_effects=True),
    )(part, tokens, mid_gain, ids, weights, blend, eg, eu, ed, dg, du, dd)


def shards(
    tokens, prior_state, first_gain, query_weight, key_weight, value_weight, decay_down, decay_up,
    decay_base, rate_down, rate_up, rate_base, head_gain, out_weight, mid_gain, route_ids,
    route_weights, expert_gate, expert_up, expert_down, dense_gate, dense_up, dense_down,
    blend_vector,
):
    part, new_state = mixer(
        tokens, prior_state, first_gain, query_weight, key_weight, value_weight, decay_down,
        decay_up, decay_base, rate_down, rate_up, rate_base, head_gain, out_weight,
    )
    top = route_ids.shape[1]
    mixed = exchange(
        part, tokens.reshape(2, ROWS, D), mid_gain.reshape(1, D), route_ids.reshape(2, ROWS, top),
        route_weights.reshape(2, ROWS, top), jnp.broadcast_to(blend_vector[None, :], (8, D)),
        expert_gate, expert_up, expert_down, dense_gate, dense_up, dense_down,
    )
    return (mixed.reshape(2 * ROWS, D // 2), new_state)


def solution(mesh):
    split = Mesh(mesh.devices.reshape(NZ, NY, NX, mesh.shape["tp"]), EP_TP)
    in_specs = (
        P(EP, None),
        P(EP, "tp", None, None),
        P(),
        P(None, "tp"),
        P(None, "tp"),
        P(None, "tp"),
        P(),
        P(None, "tp"),
        P("tp"),
        P(),
        P(None, "tp"),
        P("tp"),
        P("tp"),
        P("tp", None),
        P(),
        P(EP, None),
        P(EP, None),
        P(EP, None, "tp"),
        P(EP, None, "tp"),
        P(EP, "tp", None),
        P(None, EP_TP),
        P(None, EP_TP),
        P(EP_TP, None),
        P(),
    )
    out_specs = (P(EP, "tp"), P(EP, "tp", None, None))
    return jax.shard_map(
        shards, mesh=split, in_specs=in_specs, out_specs=out_specs, check_vma=False
    )
```

time: 298 us -> 105 us (0.35)
  waiting for transfers between devices: 111 us -> 0 us
  Pallas kernels: 0 us -> 89 us
  blocking collectives: 59.2 us -> 0 us
  starting transfers between devices: 41.4 us -> 0 us
  other arithmetic: 28.7 us -> 0 us
  matrix products: 21.4 us -> 0 us
  between operations: 14.4 us -> 0.74 us
  local copies, waits for them, and re-layouts: 20.6 us -> 14.5 us
    pallas_call x0 -> x2, Pallas kernels: none -> 89 us  [the longest x1 73.3 us: exchange(): pl.pallas_call(exchange_kernel, name='exchange', out_shape=jax.ShapeDtype...]
    all_to_all x5 -> x0, waiting for transfers between devices: 69.4 us -> none  [the longest x2 33.6 us: moved(): lax.all_to_all(group, axis, split_axis=split_dim, concat_axis=concat_dim,...]
    all_to_all x5 -> x0, starting transfers between devices: 41.3 us -> none  [the longest x2 22.5 us: moved(): lax.all_to_all(group, axis, split_axis=split_dim, concat_axis=concat_dim,...]
    all_gather x3 -> x0, waiting for transfers between devices: 41.2 us -> none  [whole_of(): value = lax.all_gather(value, axis, axis=dim, tiled=True)]
    all_gather x3 -> x0, blocking collectives: 33 us -> none  [whole_of(): value = lax.all_gather(value, axis, axis=dim, tiled=True)]
    dot_general x14 -> x0, matrix products: 21.4 us -> none  [the longest x1 5 us: shards(): jnp.dot(own_units, whole_of(dense_down, EP, 0), preferred_element_type=jn...]
    all_to_all x3 -> x0, blocking collectives: 18.6 us -> none  [summed_on_arrival(): lax.all_to_all(cut_along(value, dim, length), axis, 0, 0, tiled=True)]
    mul x5 -> x0, other arithmetic: 15.9 us -> none  [the longest x1 15.7 us: mixer_core(): removed[..., None] * (unit_key * learn_rate)[:, :, None, :]]
  transfers between devices with their start and end apart: 8 -> 0, of which waited for: 6 -> 0; matrix products, arithmetic and copies ran while one was open for 21% -> 0% of each run, Pallas kernels for 0% -> 0%
where the time goes in v1:
time: 105 us; the launch traced here: 104 us
  Pallas kernels  89 us (85%)
  local copies, waits for them, and re-layouts  14.5 us (14%)
    pallas_call x1, Pallas kernels, exchange(): pl.pallas_call(exchange_kernel, name='exchange', out_shape=jax.ShapeDtype...  73.3 us
    pallas_call x1, Pallas kernels, mixer(): pl.pallas_call(mixer_kernel, name='mixer', out_shape=(jax.ShapeDtypeStruc...  15.7 us
    unnamed x31, local copies, waits for them, and re-layouts  9.35 us

profile of v1, /device:TPU:1, one launch (start us, length us, event | category | flops | bytes accessed | tf_op | source)
XLA Modules:
  0.0 104.2 jit_solution(8126837928707945874)
XLA Ops:
  0.6 0.0 copy-start.9
  0.6 0.0 copy-start.4
  0.7 0.0 copy-start.10
  0.7 0.0 copy-start.11
  0.7 1.9 %copy.34.dd = bf16[1536,96]{1,0:T(8,128)(2,1)} copy(bf16[1536,96]{0,1:T(8,128)(2,1)} %param.30) | data formatting | bytes 589824 | tf_op args[6]
  2.6 1.9 %copy.35.rd = bf16[1536,96]{1,0:T(8,128)(2,1)} copy(bf16[1536,96]{0,1:T(8,128)(2,1)} %param.33) | data formatting | bytes 589824 | tf_op args[9]
  4.5 0.0 copy-done.9
  4.5 0.9 reshape.41.hg
  5.3 0.0 copy-done.4
  5.3 0.6 reshape.32.gain
  5.9 0.0 copy-done.10
  5.9 0.6 reshape.33.db
  6.5 0.0 copy-done.11
  6.5 0.5 reshape.34.rb
  7.1 0.0 copy-start
  7.1 15.7 %mixer.1 = (bf16[2,8,1536]{2,1,0:T(8,128)(2,1)}, f32[16,6,64,64]{3,2,1,0:T(8,128)}) custom-call(bf16[16,1536]{1,0:T(8,128)(2,1)} %tok.1, f32[1,1536]{1,0:T(1,128)} %reshape.32.gain, bf16[1536,384]{1,0:T(8,128)(2,1)} %wq_h.1, bf16[1536,384]{1,0:T(8,128)(2,1)} %wk_h.1, bf16[1536,384]{1,0:T(8,128)(2,1)} %wv_h.1, bf16[1536,96]{1,0:T(8,128)(2,1)} %copy.34.dd, ...), custom_call_target="tpu_custom_call" | custom-call | tf_op jit(solution)/shard_map/mixer/pallas_call | solution.py:123
  22.7 0.0 copy-start.1
  22.7 0.0 copy-done
  22.7 0.0 copy-start.2
  22.8 1.2 %copy.39.eg_h = bf16[1,1536,192]{2,1,0:T(8,128)(2,1)} copy(bf16[1,1536,192]{1,2,0:T(8,128)(2,1)S(1)} %copy-done) | data formatting | bytes 1179648 | tf_op args[17]
  23.9 0.0 copy-done.1
  23.9 0.0 copy-start.3
  23.9 0.0 copy-start.6
  23.9 0.0 copy-start.7
  23.9 0.0 copy-start.8
  23.9 0.0 copy-start.5
  23.9 1.2 %copy.40.eu_h = bf16[1,1536,192]{2,1,0:T(8,128)(2,1)} copy(bf16[1,1536,192]{1,2,0:T(8,128)(2,1)S(1)} %copy-done.1) | data formatting | bytes 1179648 | tf_op args[18]
  25.1 0.0 copy-done.2
  25.1 0.9 copy.41.dg_h
  26.0 0.0 copy-done.3
  26.0 0.9 copy.42.du_h
  27.0 0.0 copy-done.6
  27.0 0.6 broadcast_in_dim.2.blend
  27.6 0.0 copy-done.7
  27.6 0.7 copy.43
  28.3 0.0 copy-done.8
  28.3 0.7 copy.44
  28.9 0.0 copy-done.5
  28.9 0.6 reshape.37.gain
  29.5 73.3 %exchange.1 = bf16[2,8,768]{2,1,0:T(8,128)(2,1)} custom-call(bf16[2,8,1536]{2,1,0:T(8,128)(2,1)} %get-tuple-element.4.part, bf16[2,8,1536]{2,1,0:T(8,128)(2,1)} %bitcast.4, f32[1,1536]{1,0:T(1,128)} %reshape.37.gain, s32[2,8,6]{2,1,0:T(8,128)} %bitcast.6, f32[2,8,6]{2,1,0:T(8,128)} %bitcast.7, bf16[8,1536]{1,0:T(8,128)(2,1)} %broadcast_in_dim.2.blend, ...), custom_call_target="tpu_custom_call" | custom-call | tf_op jit(solution)/shard_map/exchange/pallas_call | solution.py:472
  102.9 1.3 %copy.46 = bf16[16,768]{1,0:T(8,128)(2,1)} copy(bf16[16,768]{1,0:T(8,128)(2,1)} %bitcast.5) | data formatting | bytes 49152
Async XLA Ops:
  0.6 3.8 %copy-start.9 = (f32[384]{0:T(512)S(1)}, f32[384]{0:T(512)}, u32[]{:S(2)}) copy-start(f32[384]{0:T(512)} %param.36) | copy-start | bytes 4612
  0.6 4.7 %copy-start.4 = (f32[1536]{0:T(1024)S(1)}, f32[1536]{0:T(1024)}, u32[]{:S(2)}) copy-start(f32[1536]{0:T(1024)} %param.26) | copy-start | bytes 18436
  0.7 5.3 %copy-start.10 = (f32[384]{0:T(512)S(1)}, f32[384]{0:T(512)}, u32[]{:S(2)}) copy-start(f32[384]{0:T(512)} %param.32) | copy-start | bytes 4612
  0.7 5.8 %copy-start.11 = (f32[384]{0:T(512)S(1)}, f32[384]{0:T(512)}, u32[]{:S(2)}) copy-start(f32[384]{0:T(512)} %param.35) | copy-start | bytes 4612
  7.1 15.7 %copy-start = (bf16[1,1536,192]{1,2,0:T(8,128)(2,1)S(1)}, bf16[1,1536,192]{1,2,0:T(8,128)(2,1)}, u32[]{:S(2)}) copy-start(bf16[1,1536,192]{1,2,0:T(8,128)(2,1)} %param.41) | copy-start | bytes 1769476
  22.7 1.2 %copy-start.1 = (bf16[1,1536,192]{1,2,0:T(8,128)(2,1)S(1)}, bf16[1,1536,192]{1,2,0:T(8,128)(2,1)}, u32[]{:S(2)}) copy-start(bf16[1,1536,192]{1,2,0:T(8,128)(2,1)} %param.42) | copy-start | bytes 1769476
  22.7 2.4 %copy-start.2 = (bf16[1536,24]{0,1:T(8,128)(2,1)S(1)}, bf16[1536,24]{0,1:T(8,128)(2,1)}, u32[]{:S(2)}) copy-start(bf16[1536,24]{0,1:T(8,128)(2,1)} %param.44) | copy-start | bytes 221188
  23.9 2.1 %copy-start.3 = (bf16[1536,24]{0,1:T(8,128)(2,1)S(1)}, bf16[1536,24]{0,1:T(8,128)(2,1)}, u32[]{:S(2)}) copy-start(bf16[1536,24]{0,1:T(8,128)(2,1)} %param.45) | copy-start | bytes 221188
  23.9 3.0 %copy-start.6 = (bf16[1536]{0:T(1024)(128)(2,1)S(1)}, bf16[1536]{0:T(1024)(128)(2,1)}, u32[]{:S(2)}) copy-start(bf16[1536]{0:T(1024)(128)(2,1)} %param.47) | copy-start | bytes 9220
  23.9 3.7 %copy-start.7 = (s32[16,6]{0,1:T(8,128)S(1)}, s32[16,6]{0,1:T(8,128)}, u32[]{:S(2)}) copy-start(s32[16,6]{0,1:T(8,128)} %param.39) | copy-start | bytes 1156
  23.9 4.3 %copy-start.8 = (f32[16,6]{0,1:T(8,128)S(1)}, f32[16,6]{0,1:T(8,128)}, u32[]{:S(2)}) copy-start(f32[16,6]{0,1:T(8,128)} %param.40) | copy-start | bytes 1156
  23.9 5.0 %copy-start.5 = (f32[1536]{0:T(1024)S(1)}, f32[1536]{0:T(1024)}, u32[]{:S(2)}) copy-start(f32[1536]{0:T(1024)} %param.38) | copy-start | bytes 18436

commit v2 on v0

v2 whole, which is shorter than its diff:
```python
import math

import jax
import jax.numpy as jnp
from jax import lax
from jax.experimental import pallas as pl
from jax.experimental.pallas import tpu as pltpu
from jax.sharding import Mesh
from jax.sharding import PartitionSpec as P

EP = ("ep_0", "ep_1", "ep_2")
EP_TP = ("ep_0", "ep_1", "ep_2", "tp")
NZ, NY, NX = 8, 4, 4
F32 = jnp.float32
BF16 = jnp.bfloat16
MESH_ID = pl.DeviceIdType.MESH
VMEM = pltpu.VMEM

D = 1536
ROWS = 8
WIDE = D + 128
AGA = slice(0, 512)
AGB = slice(512, 1024)
AGAB = slice(0, 1024)
AGC = slice(1024, WIDE)
CA = slice(0, 512)
CB = slice(512, 1024)
CC = slice(1024, 1536)
W = 512
N_SEND, N_RECV, N_TILES = 10, 117, 1152


def dot(a, b):
    return jnp.dot(a, b, preferred_element_type=F32)


def dot_t(a, b):
    return lax.dot_general(a, b, (((1,), (1,)), ((), ())), preferred_element_type=F32)


def flat(ref):
    return jnp.concatenate([ref[j : j + 1, :] for j in range(ref.shape[0])], axis=1)


scope = jax.named_scope


def mixer_kernel(
    tok, gain, wq_h, wk_h, wv_h, dd, du, db, rd, ru, rb, hg, wo_h, st_h,
    part, st_out,
    wq, wk, wv, wo, st, dec_s, left_s, right_s, val_s, both_s, wsem, isem, osem,
):
    heads = st_h.shape[1]
    rows = tok.shape[0]
    loads = [
        pltpu.make_async_copy(src, dst, wsem.at[i])
        for i, (src, dst) in enumerate(((wk_h, wk), (wv_h, wv), (wq_h, wq), (wo_h, wo)))
    ]
    for load in loads[:3]:
        load.start()
    states = [pltpu.make_async_copy(st_h.at[:, h], st.at[h], isem.at[h]) for h in range(heads)]
    for copy in states:
        copy.start()
    loads[3].start()
    with scope("m_norm"):
        token_f = tok[...].astype(F32)
        scale = lax.rsqrt(jnp.mean(token_f * token_f, axis=-1, keepdims=True) + 1e-06)
        normed = (token_f * scale * flat(gain)).astype(BF16)
        decay_low = jnp.tanh(dot_t(normed, dd[...])).astype(BF16)
        decay_in = flat(db) + dot(decay_low, du[...])
        decay = jnp.exp(-0.6065306597126334 * jax.nn.sigmoid(decay_in))
        rate_low = dot_t(normed, rd[...]).astype(BF16)
        learn = jax.nn.sigmoid(flat(rb) + dot(rate_low, ru[...]))
    with scope("m_qkv"):
        loads[0].wait()
        key = dot(normed, wk[...]).astype(BF16).astype(F32)
        loads[1].wait()
        value = dot(normed, wv[...]).astype(BF16).astype(F32)
        loads[2].wait()
        rec = dot(normed, wq[...]).astype(BF16).astype(F32)
    with scope("m_prep"):
        val_s[...] = jnp.transpose(jnp.concatenate([jnp.zeros_like(value), value], axis=0)).reshape(
            heads, 64, 2 * rows
        )
        taken, given = [], []
        for h in range(heads):
            lanes = slice(64 * h, 64 * h + 64)
            k, r, d = key[:, lanes], rec[:, lanes], decay[:, lanes]
            unit = k * lax.rsqrt(jnp.sum(k * k, axis=-1, keepdims=True) + 1e-06)
            rate = unit * learn[:, lanes]
            dec_s[h] = d
            left_s[h, 0:rows] = unit.astype(BF16)
            left_s[h, rows : 2 * rows] = (d * r).astype(BF16)
            right_s[h, 0:rows] = rate.astype(BF16)
            right_s[h, rows : 2 * rows] = k.astype(BF16)
            taken.append(jnp.sum(rate * r, axis=-1, keepdims=True))
            given.append(jnp.sum(k * r, axis=-1, keepdims=True))

    lane = lax.broadcasted_iota(jnp.int32, (64, 2 * rows), 1)

    def head(h, carry):
        pltpu.make_async_copy(st_h.at[:, h], st.at[h], isem.at[h]).wait()
        prior = st[h].reshape(rows * 64, 64)
        products = dot_t(prior.astype(BF16), left_s[h])
        own = jnp.zeros((64, 2 * rows), F32)
        values = val_s[h]
        outer = []
        for b in range(rows):
            here = products[64 * b : 64 * b + 64]
            first, second = lane == b, lane == rows + b
            own = jnp.where(first | second, here, own)
            outer.append(
                jnp.where(first, -here, jnp.where(second, values, 0.0)).astype(BF16)
            )
        change = dot(jnp.concatenate(outer, axis=0), right_s[h])
        for b in range(rows):
            part_b = slice(64 * b, 64 * b + 64)
            st[h, b] = prior[part_b] * dec_s[h, b : b + 1, :] + change[part_b]
        both_s[pl.ds(pl.multiple_of(h * 64, 64), 64), :] = own
        pltpu.make_async_copy(st.at[h], st_out.at[:, h], osem.at[h]).start()
        return carry

    with scope("m_state"):
        lax.fori_loop(0, heads, head, 0)
    with scope("m_out"):
        both = jnp.transpose(both_s[...])
        mixed = []
        for h in range(heads):
            lanes = slice(64 * h, 64 * h + 64)
            read = (
                both[rows : 2 * rows, lanes]
                - both[0:rows, lanes] * taken[h]
                + value[:, lanes] * given[h]
            )
            diff = read - jnp.mean(read, axis=-1, keepdims=True)
            spread = jnp.mean(diff * diff, axis=-1, keepdims=True)
            mixed.append(diff * lax.rsqrt(spread + 0.00064))
        mixed = (jnp.concatenate(mixed, axis=1) * flat(hg)).astype(BF16)
        loads[3].wait()
        partial = dot(mixed, wo[...])
        part[0] = partial[0:8].astype(BF16)
        part[1] = partial[8:16].astype(BF16)

    def drain(h, carry):
        pltpu.make_async_copy(st.at[h], st_out.at[:, h], osem.at[h]).wait()
        return carry

    with scope("m_drain"):
        lax.fori_loop(0, heads, drain, 0)


def mixer(tokens, prior_state, first_gain, wq, wk, wv, dd, du, db, rd, ru, rb, hg, wo):
    rows, heads = prior_state.shape[:2]
    vm = pl.BlockSpec(memory_space=VMEM)
    hbm = pl.BlockSpec(memory_space=pl.ANY)
    inner = heads * 64
    return pl.pallas_call(
        mixer_kernel,
        name="mixer",
        out_shape=(
            jax.ShapeDtypeStruct((2, rows // 2, D), BF16),
            jax.ShapeDtypeStruct(prior_state.shape, F32),
        ),
        in_specs=[vm, vm, hbm, hbm, hbm, vm, vm, vm, vm, vm, vm, vm, hbm, hbm],
        out_specs=(vm, hbm),
        scratch_shapes=[
            VMEM((D, inner), BF16), VMEM((D, inner), BF16), VMEM((D, inner), BF16),
            VMEM((inner, D), BF16), VMEM((heads, rows, 64, 64), F32),
            VMEM((heads, rows, 64), F32),
            VMEM((heads, 2 * rows, 64), BF16), VMEM((heads, 2 * rows, 64), BF16),
            VMEM((heads, 64, 2 * rows), F32), VMEM((inner, 2 * rows), F32),
            pltpu.SemaphoreType.DMA((4,)),
            pltpu.SemaphoreType.DMA((heads,)),
            pltpu.SemaphoreType.DMA((heads,)),
        ],
    )(
        tokens, first_gain.reshape(-1, 128), wq, wk, wv, dd.T, du, db.reshape(-1, 128), rd.T, ru,
        rb.reshape(-1, 128), hg.reshape(-1, 128), wo, prior_state,
    )


class Group:
    def __init__(self, index):
        self.index, self.tiles = index, 0


AROUND = (2, 1, -1, 0)
UP4, DOWN4 = (2, 1), (-1, 0)


def exchange_kernel(
    part, tok, gain, ids, weights, blend, eg_h, eu_h, ed_h, dg_h, du_h, dd_h,
    out,
    full, made, w1, w2, shares_s, peer_part, res_s, res_in,
    ax1, axf, ay1, ayf, bx1, bxf, by1, byf, a2, b2, z3, r3, cz, c2, ry, c3, rx, tiles,
    send_sem, recv_sem, load_sem,
):
    z, y, x = (lax.axis_index(a) for a in EP)
    c = lax.axis_index("tp")
    expert = (z * NY + y) * NX + x
    families, groups = [], []

    def xa(d):
        return lax.rem(x + d + NX, NX)

    def ya(d):
        return lax.rem(y + d + NY, NY)

    def za(d):
        return lax.rem(z + d + NZ, NZ)

    def dev(dx=0, dy=0, dz=0, dc=0):
        return {
            "ep_0": za(dz) if dz else z,
            "ep_1": ya(dy) if dy else y,
            "ep_2": xa(dx) if dx else x,
            "tp": 1 - c if dc else c,
        }

    def family():
        families.append(Group(len(families)))
        return families[-1]

    def group():
        groups.append(Group(len(groups)))
        return groups[-1]

    def send(src, dst, to, sent, got):
        size = math.prod(src.shape) // (ROWS * 128)
        sent.tiles += size
        got.tiles += size
        pltpu.make_async_remote_copy(
            src_ref=src, dst_ref=dst, send_sem=send_sem.at[sent.index],
            recv_sem=recv_sem.at[got.index], device_id=to, device_id_type=MESH_ID,
        ).start()
        return got

    def all_of(g):
        view = tiles.at[pl.ds(0, g.tiles)]
        return pltpu.make_async_remote_copy(
            src_ref=view, dst_ref=view,
            send_sem=send_sem.at[g.index if g in families else 0],
            recv_sem=recv_sem.at[g.index if g in groups else 0],
            device_id=dev(dc=1), device_id_type=MESH_ID,
        )

    def arrive(*some):
        for g in some:
            all_of(g).wait_recv()

    pieces = [
        (eg_h.at[0], w1.at[0, pl.ds(0, 192), :]),
        (dg_h, w1.at[0, pl.ds(192, 24), :]),
        (eu_h.at[0], w1.at[0, pl.ds(256, 192), :]),
        (du_h, w1.at[0, pl.ds(448, 24), :]),
    ]
    for k, at in enumerate((0, 768, 256, 1024, 512, 1280)):
        here, there = pl.ds(256 * k, 256), pl.ds(at, 256)
        pieces.append((ed_h.at[0, :, there], w2.at[0, pl.ds(0, 192), here]))
        pieces.append((dd_h.at[:, there], w2.at[0, pl.ds(192, 24), here]))
    loads = [pltpu.make_async_copy(src, dst, load_sem.at[i]) for i, (src, dst) in enumerate(pieces)]
    for load in loads:
        load.start()

    with scope("barrier"):
        peers = (
            [dev(dx=d, dc=e) for d in range(1, NX) for e in (0, 1)]
            + [dev(dy=d) for d in range(1, NY)]
            + [dev(dz=d, dc=e) for d in range(1, NZ) for e in (0, 1)]
            + [dev(dc=1)]
        )
        barrier = pltpu.get_barrier_semaphore()
        for peer in peers:
            pl.semaphore_signal(barrier, inc=1, device_id=peer, device_id_type=MESH_ID)
        pl.semaphore_wait(barrier, len(peers))

    near = family()
    swap = send(part.at[1 - c], peer_part, dev(dc=1), near, group())

    with scope("shares"):
        own_w = weights[...]
        share = own_w / jnp.sum(own_w, axis=0, keepdims=True) * 2.5
        sub = lax.broadcasted_iota(jnp.int32, (128, 2 * ROWS), 0)
        shares = jnp.zeros((128, 2 * ROWS), F32)
        for k in range(own_w.shape[0]):
            shares = shares + jnp.where(ids[k : k + 1, :] == sub, share[k : k + 1, :], 0.0)
        shares_s[...] = jnp.transpose(shares).reshape(2, ROWS, 128)
        full[x, y, z, :, D:WIDE] = shares_s[c].astype(BF16)
        first_row = lax.broadcasted_iota(jnp.int32, (ROWS, D), 0) == 0
        w1[0, 216:224, :] = jnp.where(first_row, blend[...].astype(F32).reshape(1, D), 0.0).astype(BF16)
        w1[0, 224:256, :] = jnp.zeros((32, D), BF16)
        w1[0, 472:512, :] = jnp.zeros((40, D), BF16)
        w2[0, 216:256, :] = jnp.zeros((40, D), BF16)

    with scope("mid"):
        arrive(swap)
        attn = part[c].astype(F32) + peer_part[...].astype(F32)
        resid_bf = (tok[c].astype(F32) + attn).astype(BF16)
        resid = resid_bf.astype(F32)
        scale = lax.rsqrt(jnp.mean(resid * resid, axis=-1, keepdims=True) + 1e-06)
        full[x, y, z, :, 0:D] = (resid * scale * flat(gain)).astype(BF16)
        res_s[0] = resid_bf[:, 0:768]
        res_s[1] = resid_bf[:, 768:1536]

    yp, ym, xp, xm = dev(dy=1), dev(dy=-1), dev(dx=1), dev(dx=-1)
    zp, zm = dev(dz=1), dev(dz=-1)
    fam_z, fam_a, fam_b, fam_c = family(), family(), family(), family()

    zab = group()
    for d in (4, 3, 5, 2, 6, 1, 7):
        ref = full.at[x, y, z, :, AGAB]
        send(ref, ref, dev(dz=d), fam_z, zab)
    cx = group()
    for d in (2, 1, 3):
        ref = full.at[x, y, z, :, AGC]
        send(ref, ref, dev(dx=d), fam_z, cx)

    resid_in = send(res_s.at[1 - c], res_in, dev(dc=1), near, group())
    with scope("w_load"):
        for load in loads:
            load.wait()
    w_fam, w_in = family(), group()
    send(w1.at[0], w1.at[1], dev(dc=1), w_fam, w_in)
    send(w2.at[0], w2.at[1], dev(dc=1), w_fam, w_in)

    def halves_out(ref_of, up, down, fam, first, rest):
        for at, half, to in ((0, 0, up), (1, 1, down), (0, 1, up), (1, 0, down)):
            ref = ref_of(0, half)
            send(ref, ref, to, fam, first[at] if half == at else rest)

    def halves_on(ref_of, up, down, fam, first, last):
        for at, d, to in ((0, -1, up), (1, 1, down)):
            arrive(first[at])
            ref = ref_of(d, at)
            send(ref, ref, to, fam, last)

    def a_y(d, half):
        return full.at[x, ya(d), pl.ds(4 * half, 4), :, AGA]

    def b_x(d, half):
        return full.at[xa(d), y, pl.ds(4 * half, 4), :, AGB]

    def a_x(j):
        return lambda d, half: full.at[xa(d), ya(j), pl.ds(4 * half, 4), :, AGA]

    def b_y(i):
        return lambda d, half: full.at[xa(i), ya(d), pl.ds(4 * half, 4), :, AGB]

    ay_first, ay_rest, ay_last = (group(), group()), group(), group()
    bx_first, bx_rest, bx_last = (group(), group()), group(), group()
    ax_first = {j: (group(), group()) for j in AROUND}
    by_first = {i: (group(), group()) for i in AROUND}
    ax_rest, by_rest = group(), group()

    def ab_out(j):
        halves_out(a_x(j), xp, xm, fam_a, ax_first[j], ax_rest)
        halves_out(b_y(j), yp, ym, fam_b, by_first[j], by_rest)

    def ab_on(j):
        halves_on(a_x(j), xp, xm, fam_a, ax_first[j], ax_rest)
        halves_on(b_y(j), yp, ym, fam_b, by_first[j], by_rest)

    up_in = {(s, q): group() for s in (1, 2, 3) for q in AROUND}
    down_in = {(s, q): group() for s in (1, 2, 3) for q in AROUND}
    c_last = group()

    def c_z(s, q):
        if s > 1:
            arrive(up_in[s - 1, q])
        if s < 4 or q in UP4:
            ref = full.at[:, ya(q), za(1 - s), :, AGC]
            send(ref, ref, zp, fam_c, up_in[s, q] if s < 4 else c_last)
        if s > 1:
            arrive(down_in[s - 1, q])
        if s < 4 or q in DOWN4:
            ref = full.at[:, ya(q), za(s - 1), :, AGC]
            send(ref, ref, zm, fam_c, down_in[s, q] if s < 4 else c_last)

    with scope("ag_cx"):
        arrive(cx)
        cy = {d: group() for d in (1, 3, 2)}
        for d in (1, 3, 2):
            ref = full.at[:, y, z, :, AGC]
            send(ref, ref, dev(dy=d), fam_c, cy[d])
        c_z(1, 0)
    with scope("ag_zab"):
        arrive(zab)
        halves_out(a_y, yp, ym, fam_a, ay_first, ay_rest)
        halves_out(b_x, xp, xm, fam_b, bx_first, bx_rest)
        ab_out(0)
    with scope("ag_cy"):
        arrive(cy[1], cy[3])
        c_z(1, 1)
        c_z(1, -1)
        arrive(cy[2])
        c_z(1, 2)
        c_z(2, 0)
    with scope("ag_ab_half"):
        halves_on(a_y, yp, ym, fam_a, ay_first, ay_last)
        halves_on(b_x, xp, xm, fam_b, bx_first, bx_last)
    with scope("ag_ab_rest"):
        arrive(ay_rest, bx_rest)
        ab_out(1)
        ab_out(-1)
        ab_on(0)
    with scope("ag_c2"):
        c_z(2, 1)
        c_z(2, -1)
        c_z(3, 0)
        c_z(2, 2)
    with scope("ag_ab_last"):
        arrive(ay_last, bx_last)
        ab_out(2)
    with scope("ag_c3"):
        c_z(3, 1)
        c_z(3, -1)
        c_z(4, 0)
    with scope("ag_ab_1"):
        ab_on(1)
        ab_on(-1)
    with scope("ag_c4"):
        c_z(3, 2)
        c_z(4, 1)
        c_z(4, -1)
    with scope("ag_ab_2"):
        ab_on(2)
    with scope("ag_c4_2"):
        c_z(4, 2)
    with scope("ag_end_ab"):
        arrive(ax_rest, by_rest)
    with scope("ag_end_c"):
        arrive(c_last, w_in)

    lane128 = lax.broadcasted_iota(jnp.int32, (256, 128), 1)
    lane256 = lax.broadcasted_iota(jnp.int32, (256, 256), 1)

    def layers(yi):
        rows_in = full[:, yi].reshape(256, WIDE)
        mid = rows_in[:, 0:D]
        chosen = jnp.sum(
            jnp.where(lane128 == expert, rows_in[:, D:WIDE].astype(F32), 0.0), axis=1, keepdims=True
        )
        both = dot_t(mid, w1[0])
        level = jnp.where(lane256 < 192, chosen, jax.nn.sigmoid(both[:, 216:217]))
        total = None
        for half in range(2):
            if half:
                both = dot_t(mid, w1[1])
            g, u = both[:, 0:256], both[:, 256:512]
            hidden = (g * jax.nn.sigmoid(g) * u * level).astype(BF16)
            term = dot(hidden, w2[half])
            total = term if total is None else total + term
        made[:, yi] = total.astype(BF16).reshape(NX, NZ, ROWS, D)

    def plus(*terms):
        total = terms[0].astype(F32)
        for term in terms[1:]:
            total = total + term.astype(F32)
        return total.astype(BF16)

    lower, upper = pl.ds(0, 4), pl.ds(4, 4)
    rs_a, rs_b, rs_c, rs_z = family(), family(), family(), family()
    slot = {j: k for k, j in enumerate(AROUND)}
    ax_one = {j: (group(), group()) for j in AROUND}
    ax_fin = {j: group() for j in AROUND}
    by_one = {i: (group(), group()) for i in AROUND}
    by_fin = {i: group() for i in AROUND}

    def a_start(j):
        k, yj = slot[j], ya(j)
        send(made.at[xa(2), yj, lower, :, CA], ax1.at[k, 0], xp, rs_a, ax_one[j][0])
        send(made.at[xa(2), yj, upper, :, CA], ax1.at[k, 1], xm, rs_a, ax_one[j][1])
        send(made.at[xa(1), yj, upper, :, CA], axf.at[k, 0, upper], xp, rs_a, ax_fin[j])
        send(made.at[xa(-1), yj, lower, :, CA], axf.at[k, 1, lower], xm, rs_a, ax_fin[j])

    def a_on(j):
        k, yj = slot[j], ya(j)
        arrive(ax_one[j][0])
        made[xa(1), yj, 0:4, :, CA] = plus(made[xa(1), yj, 0:4, :, CA], ax1[k, 0])
        send(made.at[xa(1), yj, lower, :, CA], axf.at[k, 0, lower], xp, rs_a, ax_fin[j])
        arrive(ax_one[j][1])
        made[xa(-1), yj, 4:8, :, CA] = plus(made[xa(-1), yj, 4:8, :, CA], ax1[k, 1])
        send(made.at[xa(-1), yj, upper, :, CA], axf.at[k, 1, upper], xm, rs_a, ax_fin[j])

    def a_end(j):
        k = slot[j]
        arrive(ax_fin[j])
        return plus(made[x, ya(j), :, :, CA], axf[k, 0], axf[k, 1])

    def b_start(i):
        k, xi = slot[i], xa(i)
        send(made.at[xi, ya(2), lower, :, CB], by1.at[k, 0], yp, rs_b, by_one[i][0])
        send(made.at[xi, ya(2), upper, :, CB], by1.at[k, 1], ym, rs_b, by_one[i][1])

    def b_free(i, d):
        k, xi = slot[i], xa(i)
        if d > 0:
            send(made.at[xi, ya(1), upper, :, CB], byf.at[k, 0, upper], yp, rs_b, by_fin[i])
        else:
            send(made.at[xi, ya(-1), lower, :, CB], byf.at[k, 1, lower], ym, rs_b, by_fin[i])

    def b_on(i):
        k, xi = slot[i], xa(i)
        arrive(by_one[i][0])
        made[xi, ya(1), 0:4, :, CB] = plus(made[xi, ya(1), 0:4, :, CB], by1[k, 0])
        send(made.at[xi, ya(1), lower, :, CB], byf.at[k, 0, lower], yp, rs_b, by_fin[i])
        arrive(by_one[i][1])
        made[xi, ya(-1), 4:8, :, CB] = plus(made[xi, ya(-1), 4:8, :, CB], by1[k, 1])
        send(made.at[xi, ya(-1), upper, :, CB], byf.at[k, 1, upper], ym, rs_b, by_fin[i])

    def b_end(i):
        k = slot[i]
        arrive(by_fin[i])
        return plus(made[xa(i), y, :, :, CB], byf[k, 0], byf[k, 1])

    class Second:
        def __init__(self, buf, one, fin, up, down, fam):
            self.buf, self.one, self.fin, self.up, self.down, self.fam = buf, one, fin, up, down, fam
            self.got, self.end = (group(), group()), group()

        def put(self, j, block):
            buf, k = self.buf, slot[j]
            buf[k] = block
            if j == 2:
                send(buf.at[k, lower], self.one.at[0], self.up, self.fam, self.got[0])
                send(buf.at[k, upper], self.one.at[1], self.down, self.fam, self.got[1])
            elif j == 1:
                send(buf.at[k, upper], self.fin.at[0, upper], self.up, self.fam, self.end)
            elif j == -1:
                send(buf.at[k, lower], self.fin.at[1, lower], self.down, self.fam, self.end)

        def on(self, j):
            buf, k = self.buf, slot[j]
            if j == 1:
                arrive(self.got[0])
                buf[k, 0:4] = plus(buf[k, 0:4], self.one[0])
                send(buf.at[k, lower], self.fin.at[0, lower], self.up, self.fam, self.end)
            else:
                arrive(self.got[1])
                buf[k, 4:8] = plus(buf[k, 4:8], self.one[1])
                send(buf.at[k, upper], self.fin.at[1, upper], self.down, self.fam, self.end)

        def sums(self):
            arrive(self.end)
            return plus(self.buf[slot[0]], self.fin[0], self.fin[1])

    c_up = {(s, q): group() for s in (1, 2, 3) for q in AROUND if s > 1 or q in UP4}
    c_down = {(s, q): group() for s in (1, 2, 3) for q in AROUND if s > 1 or q in DOWN4}
    c_fin = {q: group() for q in AROUND}

    def c_send(s, q, up):
        way, to = (0, zp) if up else (1, zm)
        at = za(5 - s) if up else za(s - 5)
        got = c_fin[q] if s == 4 else (c_up if up else c_down)[s, q]
        send(made.at[:, ya(q), at, :, CC], cz.at[way, s - 1, slot[q]], to, rs_c, got)

    def c_start(q):
        c_send(1, q, q in UP4)
        c_send(2, q, q in DOWN4)

    def c_on(s, q):
        for up, got in ((True, c_up), (False, c_down)):
            if (s - 1, q) in got:
                at = za(5 - s) if up else za(s - 5)
                arrive(got[s - 1, q])
                made[:, ya(q), at, :, CC] = plus(
                    made[:, ya(q), at, :, CC], cz[0 if up else 1, s - 2, slot[q]]
                )
                c_send(s, q, up)

    cy_in = group()

    def c_end(q):
        k = slot[q]
        arrive(c_fin[q])
        c2[k] = plus(made[:, ya(q), z, :, CC], cz[0, 3, k], cz[1, 3, k])
        if q:
            send(c2.at[k], ry.at[k], dev(dy=q), rs_c, cy_in)

    a_next = Second(a2, ay1, ayf, yp, ym, rs_a)
    b_next = Second(b2, bx1, bxf, xp, xm, rs_b)

    with scope("rs_m2"):
        layers(ya(2))
        a_start(2)
        c_start(2)
        for i in AROUND:
            b_start(i)
    with scope("rs_m1"):
        layers(ya(1))
        a_start(1)
        c_start(1)
        for i in AROUND:
            b_free(i, 1)
    with scope("rs_m-1"):
        layers(ya(-1))
        a_start(-1)
        c_start(-1)
        for i in AROUND:
            b_free(i, -1)
    with scope("rs_on2"):
        c_on(2, 2)
        a_on(2)
    with scope("rs_m0"):
        layers(y)
        a_start(0)
        c_start(0)
    with scope("rs_b_on"):
        c_on(3, 2)
        b_on(2)
        c_on(2, 1)
        b_on(1)
    with scope("rs_a_on"):
        a_on(1)
        c_on(2, -1)
        a_on(-1)
        b_on(-1)
        b_on(0)
    with scope("rs_c_a"):
        c_on(4, 2)
        c_on(3, 1)
        c_on(2, 0)
        c_on(3, -1)
    with scope("rs_a_end2"):
        a_next.put(2, a_end(2))
        a_on(0)
        b_next.put(2, b_end(2))
    with scope("rs_a_end1"):
        a_next.put(1, a_end(1))
        c_on(4, 1)
        c_on(3, 0)
        c_on(4, -1)
        a_next.put(-1, a_end(-1))
    with scope("rs_b_end1"):
        b_next.put(1, b_end(1))
        c_end(2)
        a_next.on(1)
        b_next.put(-1, b_end(-1))
    with scope("rs_next"):
        a_next.on(-1)
        c_on(4, 0)
        b_next.on(1)
        b_next.on(-1)
    with scope("rs_c_end"):
        c_end(1)
        c_end(-1)
    with scope("rs_ab_0"):
        a_next.put(0, a_end(0))
        b_next.put(0, b_end(0))

    z_same, z_other, x_in = group(), group(), group()
    with scope("rs_z_out"):
        sums_a = a_next.sums()
        z3[0, :, :, 0:256] = sums_a[:, :, 0:256]
        z3[1, :, :, 0:256] = sums_a[:, :, 256:512]
        sums_b = b_next.sums()
        z3[0, :, :, 256:512] = sums_b[:, :, 0:256]
        z3[1, :, :, 256:512] = sums_b[:, :, 256:512]
        for d in (4, 3, 5, 2, 6, 1, 7, 0):
            send(z3.at[1 - c, za(d)], r3.at[1, d], dev(dz=d, dc=1), rs_z, z_other)
            if d:
                send(z3.at[c, za(d)], r3.at[0, d], dev(dz=d), rs_z, z_same)
    with scope("rs_c_x"):
        c_end(0)
        arrive(cy_in)
        sums_c = plus(*(ry[slot[q]] for q in (1, -1, 2)), c2[slot[0]])
        c3[0] = sums_c[:, :, 0:256]
        c3[1] = sums_c[:, :, 256:512]
        for d in (2, 1, 3, 0):
            send(c3.at[1 - c, xa(d)], rx.at[1, d], dev(dx=d, dc=1), rs_z, x_in)
            if d:
                send(c3.at[c, xa(d)], rx.at[0, d], dev(dx=d), rs_z, x_in)
    with scope("rs_fin"):
        arrive(resid_in, z_same)
        total = res_s[c, :, 0:512].astype(F32) + z3[c, z].astype(F32)
        for d in range(1, NZ):
            total = total + r3[0, d].astype(F32)
        out[c, :, 0:512] = total.astype(BF16)
        arrive(z_other)
        total = res_in[:, 0:512].astype(F32)
        for d in range(NZ):
            total = total + r3[1, d].astype(F32)
        out[1 - c, :, 0:512] = total.astype(BF16)
        arrive(x_in)
        out[c, :, 512:768] = plus(res_s[c, :, 512:768], c3[c, x], rx[0, 1], rx[0, 2], rx[0, 3])
        out[1 - c, :, 512:768] = plus(res_in[:, 512:768], rx[1, 0], rx[1, 1], rx[1, 2], rx[1, 3])
    with scope("drain"):
        for sent in families:
            all_of(sent).wait_send()
    assert len(families) <= N_SEND and len(groups) <= N_RECV, (len(families), len(groups))
    assert max(g.tiles for g in families + groups) <= N_TILES


def exchange(part, tokens, mid_gain, ids, weights, blend, eg, eu, ed, dg, du, dd):
    vm = pl.BlockSpec(memory_space=VMEM)
    hbm = pl.BlockSpec(memory_space=pl.ANY)
    return pl.pallas_call(
        exchange_kernel,
        name="exchange",
        out_shape=jax.ShapeDtypeStruct((2, ROWS, D // 2), BF16),
        in_specs=[vm] * 6 + [hbm] * 6,
        out_specs=vm,
        scratch_shapes=[
            VMEM((NX, NY, NZ, ROWS, WIDE), BF16),
            VMEM((NX, NY, NZ, ROWS, D), BF16),
            VMEM((2, 512, D), BF16),
            VMEM((2, 256, D), BF16),
            VMEM((2, ROWS, 128), F32),
            VMEM((ROWS, D), BF16), VMEM((2, ROWS, D // 2), BF16), VMEM((ROWS, D // 2), BF16),
            VMEM((4, 2, 4, ROWS, W), BF16), VMEM((4, 2, NZ, ROWS, W), BF16),
            VMEM((2, 4, ROWS, W), BF16), VMEM((2, NZ, ROWS, W), BF16),
            VMEM((2, 4, ROWS, W), BF16), VMEM((2, NZ, ROWS, W), BF16),
            VMEM((4, 2, 4, ROWS, W), BF16), VMEM((4, 2, NZ, ROWS, W), BF16),
            VMEM((4, NZ, ROWS, W), BF16), VMEM((4, NZ, ROWS, W), BF16),
            VMEM((2, NZ, ROWS, W), BF16), VMEM((2, NZ, ROWS, W), BF16),
            VMEM((2, 4, 4, NX, ROWS, W), BF16), VMEM((4, NX, ROWS, W), BF16),
            VMEM((4, NX, ROWS, W), BF16), VMEM((2, NX, ROWS, W // 2), BF16),
            VMEM((2, NX, ROWS, W // 2), BF16),
            VMEM((N_TILES, ROWS, 128), BF16),
            pltpu.SemaphoreType.DMA((N_SEND,)),
            pltpu.SemaphoreType.DMA((N_RECV,)),
            pltpu.SemaphoreType.DMA((16,)),
        ],
        compiler_params=pltpu.CompilerParams(collective_id=0, has_side_effects=True),
    )(part, tokens, mid_gain, ids, weights, blend, eg, eu, ed, dg, du, dd)


def shards(
    tokens, prior_state, first_gain, query_weight, key_weight, value_weight, decay_down, decay_up,
    decay_base, rate_down, rate_up, rate_base, head_gain, out_weight, mid_gain, route_ids,
    route_weights, expert_gate, expert_up, expert_down, dense_gate, dense_up, dense_down,
    blend_vector,
):
    part, new_state = mixer(
        tokens, prior_state, first_gain, query_weight, key_weight, value_weight, decay_down,
        decay_up, decay_base, rate_down, rate_up, rate_base, head_gain, out_weight,
    )
    mixed = exchange(
        part, tokens.reshape(2, ROWS, D), mid_gain.reshape(-1, 128), route_ids.T, route_weights.T,
        blend_vector, jnp.swapaxes(expert_gate, 1, 2),
        jnp.swapaxes(expert_up, 1, 2), expert_down, dense_gate.T, dense_up.T, dense_down,
    )
    return (mixed.reshape(2 * ROWS, D // 2), new_state)


def solution(mesh):
    split = Mesh(mesh.devices.reshape(NZ, NY, NX, mesh.shape["tp"]), EP_TP)
    in_specs = (
        P(EP, None),
        P(EP, "tp", None, None),
        P(),
        P(None, "tp"),
        P(None, "tp"),
        P(None, "tp"),
        P(),
        P(None, "tp"),
        P("tp"),
        P(),
        P(None, "tp"),
        P("tp"),
        P("tp"),
        P("tp", None),
        P(),
        P(EP, None),
        P(EP, None),
        P(EP, None, "tp"),
        P(EP, None, "tp"),
        P(EP, "tp", None),
        P(None, EP_TP),
        P(None, EP_TP),
        P(EP_TP, None),
        P(),
    )
    out_specs = (P(EP, "tp"), P(EP, "tp", None, None))
    return jax.shard_map(
        shards, mesh=split, in_specs=in_specs, out_specs=out_specs, check_vma=False
    )
```

time: 298 us -> 77 us (0.26)
  waiting for transfers between devices: 111 us -> 0 us
  Pallas kernels: 0 us -> 74.7 us
  blocking collectives: 59.2 us -> 0 us
  starting transfers between devices: 41.4 us -> 0 us
  other arithmetic: 28.7 us -> 0 us
  matrix products: 21.4 us -> 0 us
  local copies, waits for them, and re-layouts: 20.6 us -> 1.35 us
  between operations: 14.4 us -> 0.65 us
    pallas_call x0 -> x2, Pallas kernels: none -> 74.7 us  [the longest x1 66.5 us: exchange(): pl.pallas_call(exchange_kernel, name='exchange', out_shape=jax.ShapeDtype...]
    all_to_all x5 -> x0, waiting for transfers between devices: 69.4 us -> none  [the longest x2 33.6 us: moved(): lax.all_to_all(group, axis, split_axis=split_dim, concat_axis=concat_dim,...]
    all_to_all x5 -> x0, starting transfers between devices: 41.3 us -> none  [the longest x2 22.5 us: moved(): lax.all_to_all(group, axis, split_axis=split_dim, concat_axis=concat_dim,...]
    all_gather x3 -> x0, waiting for transfers between devices: 41.2 us -> none  [whole_of(): value = lax.all_gather(value, axis, axis=dim, tiled=True)]
    all_gather x3 -> x0, blocking collectives: 33 us -> none  [whole_of(): value = lax.all_gather(value, axis, axis=dim, tiled=True)]
    dot_general x14 -> x0, matrix products: 21.4 us -> none  [the longest x1 5 us: shards(): jnp.dot(own_units, whole_of(dense_down, EP, 0), preferred_element_type=jn...]
    all_to_all x3 -> x0, blocking collectives: 18.6 us -> none  [summed_on_arrival(): lax.all_to_all(cut_along(value, dim, length), axis, 0, 0, tiled=True)]
    mul x5 -> x0, other arithmetic: 15.9 us -> none  [the longest x1 15.7 us: mixer_core(): removed[..., None] * (unit_key * learn_rate)[:, :, None, :]]
  transfers between devices with their start and end apart: 8 -> 0, of which waited for: 6 -> 0; matrix products, arithmetic and copies ran while one was open for 21% -> 0% of each run, Pallas kernels for 0% -> 0%
where the time goes in v2:
time: 77 us; the launch traced here: 76.7 us
  Pallas kernels  74.7 us (97%)
  local copies, waits for them, and re-layouts  1.35 us (2%)
    pallas_call x1, Pallas kernels, exchange(): pl.pallas_call(exchange_kernel, name='exchange', out_shape=jax.ShapeDtype...  66.5 us
    pallas_call x1, Pallas kernels, mixer(): pl.pallas_call(mixer_kernel, name='mixer', out_shape=(jax.ShapeDtypeStruc...  8.28 us

profile of v2, /device:TPU:1, one launch (start us, length us, event | category | flops | bytes accessed | tf_op | source)
XLA Modules:
  0.0 76.7 jit_solution(4943845171500723035)
XLA Ops:
  0.6 8.3 %mixer.1 = (bf16[2,8,1536]{2,1,0:T(8,128)(2,1)}, f32[16,6,64,64]{3,2,1,0:T(8,128)}) custom-call(bf16[16,1536]{1,0:T(8,128)(2,1)} %tok.1, f32[12,128]{1,0:T(8,128)} %bitcast.23, bf16[1536,384]{1,0:T(8,128)(2,1)} %wq_h.1, bf16[1536,384]{1,0:T(8,128)(2,1)} %wk_h.1, bf16[1536,384]{1,0:T(8,128)(2,1)} %wv_h.1, bf16[96,1536]{1,0:T(8,128)(2,1)} %bitcast.17, ...), custom_call_target="tpu_custom_call" | custom-call | tf_op jit(solution)/shard_map/mixer/pallas_call | solution.py:157
  8.9 66.5 %exchange.1 = bf16[2,8,768]{2,1,0:T(8,128)(2,1)} custom-call(bf16[2,8,1536]{2,1,0:T(8,128)(2,1)} %get-tuple-element.4.part, bf16[2,8,1536]{2,1,0:T(8,128)(2,1)} %bitcast.19, f32[12,128]{1,0:T(8,128)} %bitcast.24, s32[6,16]{1,0:T(8,128)} %bitcast.25, f32[6,16]{1,0:T(8,128)} %bitcast.26, bf16[1536]{0:T(1024)(128)(2,1)} %blend.1, ...), custom_call_target="tpu_custom_call" | custom-call | tf_op jit(solution)/shard_map/exchange/pallas_call | solution.py:697
  75.4 1.3 %copy.27 = bf16[16,768]{1,0:T(8,128)(2,1)} copy(bf16[16,768]{1,0:T(8,128)(2,1)} %bitcast.20) | data formatting | bytes 49152

commit v3 on v2

v3 whole, which is shorter than its diff:
```python
import math

import jax
import jax.numpy as jnp
from jax import lax
from jax.experimental import pallas as pl
from jax.experimental.pallas import tpu as pltpu
from jax.sharding import Mesh
from jax.sharding import PartitionSpec as P

EP = ("ep_0", "ep_1", "ep_2")
EP_TP = ("ep_0", "ep_1", "ep_2", "tp")
NZ, NY, NX = 8, 4, 4
F32 = jnp.float32
BF16 = jnp.bfloat16
MESH_ID = pl.DeviceIdType.MESH
VMEM = pltpu.VMEM

D = 1536
ROWS = 8
WIDE = D + 128
AGA = slice(0, 512)
AGB = slice(512, 1024)
AGAB = slice(0, 1024)
AGC = slice(1024, WIDE)
AGC_D = slice(1024, D)
CA = slice(0, 512)
CB = slice(512, 1024)
CC = slice(1024, 1536)
W = 512
N_SEND, N_RECV, N_TILES = 10, 160, 1152


def dot(a, b):
    return jnp.dot(a, b, preferred_element_type=F32)


def dot_t(a, b):
    return lax.dot_general(a, b, (((1,), (1,)), ((), ())), preferred_element_type=F32)


def flat(ref):
    return jnp.concatenate([ref[j : j + 1, :] for j in range(ref.shape[0])], axis=1)


scope = jax.named_scope


def mixer_kernel(
    tok_h, gain_h, wq_h, wk_h, wv_h, dd_h, du_h, db_h, rd_h, ru_h, rb_h, hg_h, wo_h, st_h,
    part_out, st_out,
    tok, gain, dd, du, db, rd, ru, rb, hg, part, wq, wk, wv, wo, st, dec_s, left_s, right_s, val_s, both_s, wsem, isem, osem,
):
    heads = st_h.shape[1]
    rows = tok.shape[0]
    loads = [
        pltpu.make_async_copy(src, dst, wsem.at[i])
        for i, (src, dst) in enumerate(((wk_h, wk), (wv_h, wv), (wq_h, wq), (wo_h, wo)))
    ]
    small = [
        pltpu.make_async_copy(src, dst, wsem.at[4 + i])
        for i, (src, dst) in enumerate(
            (
                (tok_h, tok), (gain_h, gain), (dd_h, dd), (rd_h, rd), (du_h, du), (ru_h, ru), (db_h, db),
                (rb_h, rb), (hg_h, hg),
            )
        )
    ]
    for load in small:
        load.start()
    for load in loads[:3]:
        load.start()
    states = [pltpu.make_async_copy(st_h.at[:, h], st.at[h], isem.at[h]) for h in range(heads)]
    for copy in states:
        copy.start()
    loads[3].start()
    with scope("m_norm"):
        for load in small:
            load.wait()
        token_f = tok[...].astype(F32)
        scale = lax.rsqrt(jnp.mean(token_f * token_f, axis=-1, keepdims=True) + 1e-06)
        normed = (token_f * scale * flat(gain)).astype(BF16)
        decay_low = jnp.tanh(dot_t(normed, dd[...])).astype(BF16)
        decay_in = flat(db) + dot(decay_low, du[...])
        decay = jnp.exp(-0.6065306597126334 * jax.nn.sigmoid(decay_in))
        rate_low = dot_t(normed, rd[...]).astype(BF16)
        learn = jax.nn.sigmoid(flat(rb) + dot(rate_low, ru[...]))
    with scope("m_qkv"):
        loads[0].wait()
        key = dot(normed, wk[...]).astype(BF16).astype(F32)
        loads[1].wait()
        value = dot(normed, wv[...]).astype(BF16).astype(F32)
        loads[2].wait()
        rec = dot(normed, wq[...]).astype(BF16).astype(F32)
    with scope("m_prep"):
        val_s[...] = jnp.transpose(jnp.concatenate([jnp.zeros_like(value), value], axis=0)).reshape(
            heads, 64, 2 * rows
        )
        taken, given = [], []
        for h in range(heads):
            lanes = slice(64 * h, 64 * h + 64)
            k, r, d = key[:, lanes], rec[:, lanes], decay[:, lanes]
            unit = k * lax.rsqrt(jnp.sum(k * k, axis=-1, keepdims=True) + 1e-06)
            rate = unit * learn[:, lanes]
            dec_s[h] = d
            left_s[h, 0:rows] = unit.astype(BF16)
            left_s[h, rows : 2 * rows] = (d * r).astype(BF16)
            right_s[h, 0:rows] = rate.astype(BF16)
            right_s[h, rows : 2 * rows] = k.astype(BF16)
            taken.append(jnp.sum(rate * r, axis=-1, keepdims=True))
            given.append(jnp.sum(k * r, axis=-1, keepdims=True))

    lane = lax.broadcasted_iota(jnp.int32, (64, 2 * rows), 1)

    def head(h, carry):
        pltpu.make_async_copy(st_h.at[:, h], st.at[h], isem.at[h]).wait()
        prior = st[h].reshape(rows * 64, 64)
        products = dot_t(prior.astype(BF16), left_s[h])
        own = jnp.zeros((64, 2 * rows), F32)
        values = val_s[h]
        outer = []
        for b in range(rows):
            here = products[64 * b : 64 * b + 64]
            first, second = lane == b, lane == rows + b
            own = jnp.where(first | second, here, own)
            outer.append(
                jnp.where(first, -here, jnp.where(second, values, 0.0)).astype(BF16)
            )
        change = dot(jnp.concatenate(outer, axis=0), right_s[h])
        for b in range(rows):
            part_b = slice(64 * b, 64 * b + 64)
            st[h, b] = prior[part_b] * dec_s[h, b : b + 1, :] + change[part_b]
        both_s[pl.ds(pl.multiple_of(h * 64, 64), 64), :] = own
        pltpu.make_async_copy(st.at[h], st_out.at[:, h], osem.at[h]).start()
        return carry

    with scope("m_state"):
        lax.fori_loop(0, heads, head, 0)
    with scope("m_out"):
        both = jnp.transpose(both_s[...])
        mixed = []
        for h in range(heads):
            lanes = slice(64 * h, 64 * h + 64)
            read = (
                both[rows : 2 * rows, lanes]
                - both[0:rows, lanes] * taken[h]
                + value[:, lanes] * given[h]
            )
            diff = read - jnp.mean(read, axis=-1, keepdims=True)
            spread = jnp.mean(diff * diff, axis=-1, keepdims=True)
            mixed.append(diff * lax.rsqrt(spread + 0.00064))
        mixed = (jnp.concatenate(mixed, axis=1) * flat(hg)).astype(BF16)
        loads[3].wait()
        partial = dot(mixed, wo[...])
        part[0] = partial[0:8].astype(BF16)
        part[1] = partial[8:16].astype(BF16)
        sent = pltpu.make_async_copy(part, part_out, wsem.at[4 + len(small)])
        sent.start()

    def drain(h, carry):
        pltpu.make_async_copy(st.at[h], st_out.at[:, h], osem.at[h]).wait()
        return carry

    with scope("m_drain"):
        lax.fori_loop(0, heads, drain, 0)
        sent.wait()


def mixer(tokens, prior_state, first_gain, wq, wk, wv, dd, du, db, rd, ru, rb, hg, wo):
    rows, heads = prior_state.shape[:2]
    hbm = pl.BlockSpec(memory_space=pl.ANY)
    inner = heads * 64
    return pl.pallas_call(
        mixer_kernel,
        name="mixer",
        out_shape=(
            jax.ShapeDtypeStruct((2, rows // 2, D), BF16),
            jax.ShapeDtypeStruct(prior_state.shape, F32),
        ),
        in_specs=[hbm] * 14,
        out_specs=(hbm, hbm),
        scratch_shapes=[
            VMEM((rows, D), BF16), VMEM((D // 128, 128), F32),
            VMEM(dd.shape[::-1], BF16), VMEM(du.shape, BF16), VMEM((inner // 128, 128), F32),
            VMEM(rd.shape[::-1], BF16), VMEM(ru.shape, BF16), VMEM((inner // 128, 128), F32),
            VMEM((inner // 128, 128), F32), VMEM((2, rows // 2, D), BF16),
            VMEM((D, inner), BF16), VMEM((D, inner), BF16), VMEM((D, inner), BF16),
            VMEM((inner, D), BF16), VMEM((heads, rows, 64, 64), F32),
            VMEM((heads, rows, 64), F32),
            VMEM((heads, 2 * rows, 64), BF16), VMEM((heads, 2 * rows, 64), BF16),
            VMEM((heads, 64, 2 * rows), F32), VMEM((inner, 2 * rows), F32),
            pltpu.SemaphoreType.DMA((14,)),
            pltpu.SemaphoreType.DMA((heads,)),
            pltpu.SemaphoreType.DMA((heads,)),
        ],
    )(
        tokens, first_gain.reshape(-1, 128), wq, wk, wv, dd.T, du, db.reshape(-1, 128), rd.T, ru,
        rb.reshape(-1, 128), hg.reshape(-1, 128), wo, prior_state,
    )


class Group:
    def __init__(self, index, copies=None):
        self.index, self.copies, self.tiles, self.sent = index, copies, 0, 0
        self.time, self.waited = 0.0, False


RATE = 46600.0
V1 = V2 = V3 = V3R = True
V4 = V4R = False
ORDER = (0, 1, 2, -1)
Z_ORDER = (4, 3, -3, 2, -2, 1, -1)
NEAR_RATE = 600000.0
START, HOP = 1.8, 0.85


class Plan:
    def __init__(self, arrive):
        self.arrive, self.now, self.links, self.steps = arrive, 0.0, {}, []

    def add(self, run, needs=(), after=(), cost=0.03, rank=5):
        step = dict(run=run, needs=needs, after=after, cost=cost, rank=rank, done=False, at=len(self.steps))
        self.steps.append(step)
        return step

    def sending(self, got, size, hops):
        begin = self.now
        end = begin + (0.0 if any(hops) else size / NEAR_RATE)
        for axis, hop in enumerate(hops):
            length = (NX, NY, NZ)[axis]
            ways = (1, -1) if 2 * abs(hop) == length else (1 if hop > 0 else -1,)
            for way in ways if hop else ():
                busy = max(begin, self.links.get((axis, way), 0.0)) + size * abs(hop) / len(ways) / RATE
                self.links[axis, way] = busy
                end = max(end, busy)
        got.sent += 1
        got.time = max(got.time, end + START + HOP * sum(abs(hop) for hop in hops))

    def run(self):
        waiting = list(self.steps)
        while waiting:
            open_ = [
                t for t in waiting
                if all(u["done"] for u in t["after"])
                and all(g.sent == g.copies for g in t["needs"])
            ]

            def when(t):
                return max([self.now] + [g.time for g in t["needs"] if not g.waited])

            step = min(open_, key=lambda t: (when(t), t["rank"], t["at"]))
            self.now = when(step) + step["cost"]
            for g in step["needs"]:
                if not g.waited:
                    self.arrive(g)
                    g.waited = True
            step["run"]()
            step["done"], step["end"] = True, self.now
            waiting.remove(step)


AROUND = (2, 1, -1, 0)
UP4, DOWN4 = (2, 1), (-1, 0)


def exchange_kernel(
    part_h, tok_h, gain_h, ids_h, weights_h, blend_h, eg_h, eu_h, ed_h, dg_h, du_h, dd_h,
    out,
    part, tok, gain, ids, weights, blend, full, made, w1, w2, shares_s, sums_s, peer_part, res_s, res_in,
    ax1, axf, ay1, ayf, bx1, bxf, by1, byf, a2, b2, z3, r3, cz, c2, ry, c3, rx, ry_a, rx_b, rxy, c4, czn, czf, tiles,
    send_sem, recv_sem, load_sem,
):
    z, y, x = (lax.axis_index(a) for a in EP)
    c = lax.axis_index("tp")
    expert = (z * NY + y) * NX + x
    families, groups = [], []

    def xa(d):
        return lax.rem(x + d + NX, NX)

    def ya(d):
        return lax.rem(y + d + NY, NY)

    def za(d):
        return lax.rem(z + d + NZ, NZ)

    def dev(dx=0, dy=0, dz=0, dc=0):
        return {
            "ep_0": za(dz) if dz else z,
            "ep_1": ya(dy) if dy else y,
            "ep_2": xa(dx) if dx else x,
            "tp": 1 - c if dc else c,
        }

    def family():
        families.append(Group(len(families)))
        return families[-1]

    def group(copies=1):
        return Group(None, copies)

    def send(src, dst, place, sent, got):
        if got.index is None:
            got.index = len(groups)
            groups.append(got)
        size = math.prod(src.shape) // (ROWS * 128)
        sent.tiles += size
        got.tiles += size
        place = dict(place)
        plan.sending(got, size * 2048, [place.get(k, 0) for k in ("dx", "dy", "dz")])
        to = dev(**place)
        pltpu.make_async_remote_copy(
            src_ref=src, dst_ref=dst, send_sem=send_sem.at[sent.index],
            recv_sem=recv_sem.at[got.index], device_id=to, device_id_type=MESH_ID,
        ).start()
        return got

    def all_of(g):
        view = tiles.at[pl.ds(0, g.tiles)]
        return pltpu.make_async_remote_copy(
            src_ref=view, dst_ref=view,
            send_sem=send_sem.at[g.index if g in families else 0],
            recv_sem=recv_sem.at[g.index if g in groups else 0],
            device_id=dev(dc=1), device_id_type=MESH_ID,
        )

    def arrive(*some):
        for g in some:
            assert g.sent == g.copies
            all_of(g).wait_recv()

    plan = Plan(arrive)

    first = [
        pltpu.make_async_copy(src, dst, load_sem.at[16 + i])
        for i, (src, dst) in enumerate(
            (
                (ids_h, ids), (weights_h, weights), (blend_h, blend), (part_h, part), (tok_h, tok), (gain_h, gain),
            )
        )
    ]
    for load in first:
        load.start()
    pieces = [
        (eg_h.at[0], w1.at[0, pl.ds(0, 192), :]),
        (dg_h, w1.at[0, pl.ds(192, 24), :]),
        (eu_h.at[0], w1.at[0, pl.ds(256, 192), :]),
        (du_h, w1.at[0, pl.ds(448, 24), :]),
    ]
    for k, at in enumerate((0, 768, 256, 1024, 512, 1280)):
        here, there = pl.ds(256 * k, 256), pl.ds(at, 256)
        pieces.append((ed_h.at[0, :, there], w2.at[0, pl.ds(0, 192), here]))
        pieces.append((dd_h.at[:, there], w2.at[0, pl.ds(192, 24), here]))
    loads = [pltpu.make_async_copy(src, dst, load_sem.at[i]) for i, (src, dst) in enumerate(pieces)]
    for load in loads:
        load.start()

    with scope("barrier"):
        peers = (
            [
                dev(dx=d, dy=f, dc=e)
                for d in range(NX) for f in range(NY) for e in (0, 1)
                if d or f or e
            ]
            + [dev(dz=d, dc=e) for d in range(1, NZ) for e in (0, 1)]
        )
        barrier = pltpu.get_barrier_semaphore()
        for peer in peers:
            pl.semaphore_signal(barrier, inc=1, device_id=peer, device_id_type=MESH_ID)
    with scope("shares"):
        for load in first:
            load.wait()
        own_w = weights[...]
        share = own_w / jnp.sum(own_w, axis=0, keepdims=True) * 2.5
        sub = lax.broadcasted_iota(jnp.int32, (128, 2 * ROWS), 0)
        shares = jnp.zeros((128, 2 * ROWS), F32)
        for k in range(own_w.shape[0]):
            shares = shares + jnp.where(ids[k : k + 1, :] == sub, share[k : k + 1, :], 0.0)
        shares_s[...] = jnp.transpose(shares).reshape(2, ROWS, 128)
        full[x, y, z, :, D:WIDE] = shares_s[c].astype(BF16)
        first_row = lax.broadcasted_iota(jnp.int32, (ROWS, D), 0) == 0
        w1[0, 216:224, :] = jnp.where(first_row, blend[...].astype(F32).reshape(1, D), 0.0).astype(BF16)
        w1[0, 224:256, :] = jnp.zeros((32, D), BF16)
        w1[0, 472:512, :] = jnp.zeros((40, D), BF16)
        w2[0, 216:256, :] = jnp.zeros((40, D), BF16)

    with scope("wait_all"):
        pl.semaphore_wait(barrier, len(peers))
    near = family()
    swap = send(part.at[1 - c], peer_part, dict(dc=1), near, group())

    with scope("mid"):
        arrive(swap)
        attn = part[c].astype(F32) + peer_part[...].astype(F32)
        resid_bf = (tok[c].astype(F32) + attn).astype(BF16)
        resid = resid_bf.astype(F32)
        scale = lax.rsqrt(jnp.mean(resid * resid, axis=-1, keepdims=True) + 1e-06)
        full[x, y, z, :, 0:D] = (resid * scale * flat(gain)).astype(BF16)
        res_s[0] = resid_bf[:, 0:768]
        res_s[1] = resid_bf[:, 768:1536]

    yp, ym, xp, xm = dict(dy=1), dict(dy=-1), dict(dx=1), dict(dx=-1)
    zp, zm = dict(dz=1), dict(dz=-1)
    fam_z, fam_a, fam_b, fam_c = family(), family(), family(), family()

    zab = group(7)
    for d in Z_ORDER:
        ref = full.at[x, y, z, :, AGAB]
        send(ref, ref, dict(dz=d), fam_z, zab)
    cx = group(3)
    cxy = {q: group(4 if q else 3) for q in AROUND}
    ref = full.at[x, y, z, :, AGC]
    if V3:
        for d in AROUND:
            for q in (2, 1, -1, 0):
                if d or q:
                    send(ref, ref, dict(dx=d, dy=q), fam_z, cxy[-q if q != 2 else 2])
    else:
        for d in (2, 1, -1):
            send(ref, ref, dict(dx=d), fam_z, cx)

    resid_in = group()
    send(res_s.at[1 - c], res_in, dict(dc=1), near, resid_in)
    with scope("w_load"):
        for load in loads:
            load.wait()
    w_fam, w_in = family(), group(2)
    send(w1.at[0], w1.at[1], dict(dc=1), w_fam, w_in)
    send(w2.at[0], w2.at[1], dict(dc=1), w_fam, w_in)

    def halves_out(ref_of, up, down, fam, first, rest):
        for at, half, to in ((0, 0, up), (1, 1, down), (0, 1, up), (1, 0, down)):
            ref = ref_of(0, half)
            send(ref, ref, to, fam, first[at] if half == at else rest[at])

    def halves_on(ref_of, up, down, fam, first, last):
        def on(at, d, to):
            def run():
                ref = ref_of(d, at)
                send(ref, ref, to, fam, last)

            return run

        return [
            plan.add(on(at, d, to), needs=[first[at]], after=[], rank=2)
            for at, d, to in ((0, -1, up), (1, 1, down))
        ]

    def a_y(d, half):
        return full.at[x, ya(d), pl.ds(4 * half, 4), :, AGA]

    def b_x(d, half):
        return full.at[xa(d), y, pl.ds(4 * half, 4), :, AGB]

    def a_x(j):
        return lambda d, half: full.at[xa(d), ya(j), pl.ds(4 * half, 4), :, AGA]

    def b_y(i):
        return lambda d, half: full.at[xa(i), ya(d), pl.ds(4 * half, 4), :, AGB]

    ay_first, ay_rest, ay_last = (group(), group()), (group(), group()), group(2)
    bx_first, bx_rest, bx_last = (group(), group()), (group(), group()), group(2)
    ax_first = {j: (group(), group()) for j in AROUND}
    by_first = {i: (group(), group()) for i in AROUND}
    ax_rest = {j: group(2) for j in AROUND}
    ax_last = {j: group(2) for j in AROUND}
    by_rest, by_last = (group(4), group(4)), group(8)

    def first_out():
        halves_out(a_y, yp, ym, fam_a, ay_first, ay_rest)
        halves_out(b_x, xp, xm, fam_b, bx_first, bx_rest)

    def a_out(j):
        return lambda: halves_out(a_x(j), xp, xm, fam_a, ax_first[j], (ax_rest[j], ax_rest[j]))

    def b_out(i):
        return lambda: halves_out(b_y(i), yp, ym, fam_b, by_first[i], by_rest)

    ay_in = {j: group() for j in (1, -1, 2)}
    bx_in = {j: group() for j in (1, -1, 2)}

    def direct_out():
        ref = full.at[x, y, :, :, AGA]
        for d in (2, 1, -1):
            send(ref, ref, dict(dy=d), fam_a, ay_in[d])
        ref = full.at[x, y, :, :, AGB]
        for d in (2, 1, -1):
            send(ref, ref, dict(dx=d), fam_b, bx_in[d])

    if V1:
        plan.add(direct_out, needs=[zab], rank=0)
    else:
        plan.add(first_out, needs=[zab], rank=0)
        halves_on(a_y, yp, ym, fam_a, ay_first, ay_last)
        halves_on(b_x, xp, xm, fam_b, bx_first, bx_last)
    for j, at in ((0, None), (1, 1), (-1, 0), (2, 2)):
        a_needs = [zab] if at is None else [ay_last] if at == 2 else [ay_first[at], ay_rest[at]]
        b_needs = [zab] if at is None else [bx_last] if at == 2 else [bx_first[at], bx_rest[at]]
        if V1 and j:
            a_needs, b_needs = [ay_in[-j if j != 2 else 2]], [bx_in[-j if j != 2 else 2]]
        plan.add(a_out(j), needs=a_needs, rank=3)
        plan.add(b_out(j), needs=b_needs, rank=3)
        halves_on(a_x(j), xp, xm, fam_a, ax_first[j], ax_last[j])
        halves_on(b_y(j), yp, ym, fam_b, by_first[j], by_last)

    up_in = {(t, q): group() for t in (1, 2, 3) for q in AROUND}
    down_in = {(t, q): group() for t in (1, 2, 3) for q in AROUND}
    c_last = {q: group() for q in AROUND}

    two_in = {(q, up): group() for q in AROUND for up in (True, False)}
    z_rest = {q: group(5) for q in AROUND}

    def c_near(q, up):
        def run():
            ref = full.at[:, ya(q), z, :, AGC]
            send(ref, ref, dict(dz=2 if up else -2), fam_c, two_in[q, up])
            send(ref, ref, dict(dz=1 if up else -1), fam_c, z_rest[q])

        return run

    def c_far(q, up):
        def run():
            ref = full.at[:, ya(q), za(-2 if up else 2), :, AGC]
            if q in (UP4 if up else DOWN4):
                send(ref, ref, dict(dz=2 if up else -2), fam_c, z_rest[q])
            send(ref, ref, dict(dz=1 if up else -1), fam_c, z_rest[q])

        return run

    def c_z(t, q, up):
        def run():
            ref = full.at[:, ya(q), za(1 - t if up else t - 1), :, AGC]
            got = c_last[q] if t == 4 else (up_in if up else down_in)[t, q]
            send(ref, ref, zp if up else zm, fam_c, got)

        return run

    cy = {1: group(2), 2: group()}

    def c_out():
        for d in (2, 1, -1):
            ref = full.at[:, y, z, :, AGC]
            send(ref, ref, dict(dy=d), fam_c, cy[abs(d)])

    if not V3:
        plan.add(c_out, needs=[cx], rank=0)
    for q in (0, 1, -1, 2):
        for up in (True, False):
            c_needs = [cxy[q]] if V3 else [cy[abs(q)] if q else cx]
            if V4:
                plan.add(c_near(q, up), needs=c_needs, rank=1)
                plan.add(c_far(q, up), needs=[two_in[q, up]], rank=1)
                continue
            plan.add(c_z(1, q, up), needs=c_needs, rank=1)
            got = up_in if up else down_in
            for t in (2, 3, 4):
                if t < 4 or q in (UP4 if up else DOWN4):
                    plan.add(c_z(t, q, up), needs=[got[t - 1, q]], rank=1)

    slot = {j: k for k, j in enumerate(AROUND)}
    lane128 = lax.broadcasted_iota(jnp.int32, (256, 128), 1)
    lane256 = lax.broadcasted_iota(jnp.int32, (256, 256), 1)

    begun = set()

    def part_of(j, cols):
        def run():
            mid = full[:, ya(j), :, :, cols].reshape(256, cols.stop - cols.start)
            for half in range(2):
                term = dot_t(mid, w1[half, :, cols])
                sums_s[slot[j], half] = sums_s[slot[j], half] + term if j in begun else term
            begun.add(j)

        return run

    def made_of(j):
        def run():
            chosen = full[:, ya(j), :, :, D:WIDE].reshape(256, 128).astype(F32)
            chosen = jnp.sum(jnp.where(lane128 == expert, chosen, 0.0), axis=1, keepdims=True)
            level = jnp.where(lane256 < 192, chosen, jax.nn.sigmoid(sums_s[slot[j], 0, :, 216:217]))
            total = None
            for half in range(2):
                g, u = sums_s[slot[j], half, :, 0:256], sums_s[slot[j], half, :, 256:512]
                hidden = (g * jax.nn.sigmoid(g) * u * level).astype(BF16)
                term = dot(hidden, w2[half])
                total = term if total is None else total + term
            made[:, ya(j)] = total.astype(BF16).reshape(NX, NZ, ROWS, D)

        return run

    every = lambda q: [two_in[q, True], two_in[q, False], z_rest[q]] if V4 else [up_in[t, q] for t in (1, 2, 3)] + [down_in[t, q] for t in (1, 2, 3)] + [c_last[q]]
    row_needs = {
        0: list(bx_in.values()) if V1 else [*bx_first, *bx_rest, bx_last],
        1: [by_rest[1]] + [by_first[i][1] for i in AROUND],
        -1: [by_rest[0]] + [by_first[i][0] for i in AROUND],
        2: [by_last],
    }
    layer = {}
    for rank, j in enumerate(ORDER):
        a_part = plan.add(
            part_of(j, AGA), needs=[w_in, *ax_first[j], ax_rest[j], ax_last[j]],
            cost=0.37, rank=20 + rank,
        )
        b_part = plan.add(part_of(j, AGB), needs=[w_in, *row_needs[j]], cost=0.37, rank=20 + rank)
        c_part = plan.add(part_of(j, AGC_D), needs=[w_in, *every(j)], cost=0.37, rank=20 + rank)
        layer[j] = plan.add(
            made_of(j), needs=every(j), after=[a_part, b_part, c_part], cost=0.65, rank=10 + rank
        )

    def plus(*terms):
        total = terms[0].astype(F32)
        for term in terms[1:]:
            total = total + term.astype(F32)
        return total.astype(BF16)

    lower, upper = pl.ds(0, 4), pl.ds(4, 4)
    rs_a, rs_b, rs_c, rs_z = family(), family(), family(), family()
    ax_one = {j: (group(), group()) for j in AROUND}
    ax_fin = {j: group(4) for j in AROUND}
    by_one = {i: (group(), group()) for i in AROUND}
    by_fin = {i: group(4) for i in AROUND}

    def a_start(j):
        def run():
            k, yj = slot[j], ya(j)
            send(made.at[xa(2), yj, lower, :, CA], ax1.at[k, 0], xp, rs_a, ax_one[j][0])
            send(made.at[xa(2), yj, upper, :, CA], ax1.at[k, 1], xm, rs_a, ax_one[j][1])
            send(made.at[xa(1), yj, upper, :, CA], axf.at[k, 0, upper], xp, rs_a, ax_fin[j])
            send(made.at[xa(-1), yj, lower, :, CA], axf.at[k, 1, lower], xm, rs_a, ax_fin[j])

        return run

    def a_on(j, at):
        def run():
            k, yj = slot[j], ya(j)
            if at == 0:
                made[xa(1), yj, 0:4, :, CA] = plus(made[xa(1), yj, 0:4, :, CA], ax1[k, 0])
                send(made.at[xa(1), yj, lower, :, CA], axf.at[k, 0, lower], xp, rs_a, ax_fin[j])
            else:
                made[xa(-1), yj, 4:8, :, CA] = plus(made[xa(-1), yj, 4:8, :, CA], ax1[k, 1])
                send(made.at[xa(-1), yj, upper, :, CA], axf.at[k, 1, upper], xm, rs_a, ax_fin[j])

        return run

    def a_end(j):
        return plus(made[x, ya(j), :, :, CA], axf[slot[j], 0], axf[slot[j], 1])

    def b_start(i):
        def run():
            k, xi = slot[i], xa(i)
            send(made.at[xi, ya(2), lower, :, CB], by1.at[k, 0], yp, rs_b, by_one[i][0])
            send(made.at[xi, ya(2), upper, :, CB], by1.at[k, 1], ym, rs_b, by_one[i][1])

        return run

    def b_free(i, d):
        def run():
            k, xi = slot[i], xa(i)
            if d > 0:
                send(made.at[xi, ya(1), upper, :, CB], byf.at[k, 0, upper], yp, rs_b, by_fin[i])
            else:
                send(made.at[xi, ya(-1), lower, :, CB], byf.at[k, 1, lower], ym, rs_b, by_fin[i])

        return run

    def b_on(i, at):
        def run():
            k, xi = slot[i], xa(i)
            if at == 0:
                made[xi, ya(1), 0:4, :, CB] = plus(made[xi, ya(1), 0:4, :, CB], by1[k, 0])
                send(made.at[xi, ya(1), lower, :, CB], byf.at[k, 0, lower], yp, rs_b, by_fin[i])
            else:
                made[xi, ya(-1), 4:8, :, CB] = plus(made[xi, ya(-1), 4:8, :, CB], by1[k, 1])
                send(made.at[xi, ya(-1), upper, :, CB], byf.at[k, 1, upper], ym, rs_b, by_fin[i])

        return run

    def b_end(i):
        return plus(made[xa(i), y, :, :, CB], byf[slot[i], 0], byf[slot[i], 1])

    def second(blocks, buf, one, fin, up, down, fam, all_in):
        got, end = (group(), group()), group(4)
        put = {}
        for j in AROUND:
            block, needs, after = blocks(j)

            def run(j=j, block=block):
                k = slot[j]
                buf[k] = block(j)
                if V2:
                    if j:
                        send(buf.at[k], all_in.at[k], dict(zip(("dy" if "dy" in up else "dx",), (j,))), fam, end)
                elif j == 2:
                    send(buf.at[k, lower], one.at[0], up, fam, got[0])
                    send(buf.at[k, upper], one.at[1], down, fam, got[1])
                elif j == 1:
                    send(buf.at[k, upper], fin.at[0, upper], up, fam, end)
                elif j == -1:
                    send(buf.at[k, lower], fin.at[1, lower], down, fam, end)

            put[j] = plan.add(run, needs=needs, after=after, cost=0.1, rank=3)
        if V2:
            end.copies = 3
            return end, put[0]

        def on_up():
            k = slot[1]
            buf[k, 0:4] = plus(buf[k, 0:4], one[0])
            send(buf.at[k, lower], fin.at[0, lower], up, fam, end)

        def on_down():
            k = slot[-1]
            buf[k, 4:8] = plus(buf[k, 4:8], one[1])
            send(buf.at[k, upper], fin.at[1, upper], down, fam, end)

        plan.add(on_up, needs=[got[0]], after=[put[1]], cost=0.06, rank=2)
        plan.add(on_down, needs=[got[1]], after=[put[-1]], cost=0.06, rank=2)
        return end, put[0]

    c_up = {(t, q): group() for t in (1, 2, 3) for q in AROUND if t > 1 or q in UP4}
    c_down = {(t, q): group() for t in (1, 2, 3) for q in AROUND if t > 1 or q in DOWN4}
    c_fin = {q: group(4 if V4R else 2) for q in AROUND}

    def c_send(t, q, up):
        way, to = (0, zp) if up else (1, zm)
        at = za(5 - t) if up else za(t - 5)
        got = c_fin[q] if t == 4 else (c_up if up else c_down)[t, q]
        send(made.at[:, ya(q), at, :, CC], cz.at[way, t - 1, slot[q]], to, rs_c, got)

    def c_start(q):
        def run():
            c_send(1, q, q in UP4)
            c_send(2, q, q in DOWN4)

        return run

    c_three = {(q, up): group(2 if q in (UP4 if up else DOWN4) else 1) for q in AROUND for up in (True, False)}

    def c_first(q):
        def run():
            k = slot[q]
            for up in (True, False):
                way, sign = (0, 1) if up else (1, -1)
                if q in (UP4 if up else DOWN4):
                    send(made.at[:, ya(q), za(4), :, CC], czf.at[way, 1, k], dict(dz=2 * sign), rs_c, c_three[q, up])
                send(made.at[:, ya(q), za(3 * sign), :, CC], czf.at[way, 0, k], dict(dz=sign), rs_c, c_three[q, up])
                send(made.at[:, ya(q), za(sign), :, CC], czn.at[way, k], dict(dz=sign), rs_c, c_fin[q])

        return run

    def c_sum(q, up):
        def run():
            k = slot[q]
            way, sign = (0, 1) if up else (1, -1)
            at = za(2 * sign)
            terms = [made[:, ya(q), at, :, CC], czf[way, 0, k]]
            if q in (UP4 if up else DOWN4):
                terms.append(czf[way, 1, k])
            made[:, ya(q), at, :, CC] = plus(*terms)
            send(made.at[:, ya(q), at, :, CC], czn.at[2 + way, k], dict(dz=2 * sign), rs_c, c_fin[q])

        return run

    def c_on(t, q, up):
        def run():
            at = za(5 - t) if up else za(t - 5)
            made[:, ya(q), at, :, CC] = plus(
                made[:, ya(q), at, :, CC], cz[0 if up else 1, t - 2, slot[q]]
            )
            c_send(t, q, up)

        return run

    cy_in = group(3)
    xy_same, xy_other = group(15), group(16)

    def c_end(q):
        def run():
            k = slot[q]
            if V4R:
                sums = plus(made[:, ya(q), z, :, CC], czn[0, k], czn[1, k], czn[2, k], czn[3, k])
            else:
                sums = plus(made[:, ya(q), z, :, CC], cz[0, 3, k], cz[1, 3, k])
            if V3R:
                c4[k, 0] = sums[:, :, 0:256]
                c4[k, 1] = sums[:, :, 256:512]
                for d in AROUND:
                    i = (d + NX) % NX
                    send(c4.at[k, 1 - c, xa(d)], rxy.at[1, k, i], dict(dx=d, dy=q, dc=1), rs_z, xy_other)
                    if d or q:
                        send(c4.at[k, c, xa(d)], rxy.at[0, k, i], dict(dx=d, dy=q), rs_z, xy_same)
                return
            c2[k] = sums
            if q:
                send(c2.at[k], ry.at[k], dict(dy=q), rs_c, cy_in)

        return run

    c_ends = []
    for j in AROUND:
        if V4R:
            begun = plan.add(c_first(j), after=[layer[j]], rank=0)
            for up in (True, False):
                plan.add(c_sum(j, up), needs=[c_three[j, up]], after=[begun], cost=0.08, rank=1)
        else:
            plan.add(c_start(j), after=[layer[j]], rank=0)
        a_begun = plan.add(a_start(j), after=[layer[j]], rank=1)
        for at in (0, 1):
            plan.add(a_on(j, at), needs=[ax_one[j][at]], after=[a_begun], cost=0.06, rank=2)
        for up, got in ((True, c_up), (False, c_down)):
            for t in () if V4R else (2, 3, 4):
                if (t - 1, j) in got:
                    plan.add(c_on(t, j, up), needs=[got[t - 1, j]], after=[layer[j]], cost=0.06, rank=1)
        c_ends.append(plan.add(c_end(j), needs=[c_fin[j]], after=[layer[j]], cost=0.08, rank=1))
        plan.add(b_start(j), after=[layer[2]], rank=1)
        for d in (1, -1):
            plan.add(b_free(j, d), after=[layer[d]], rank=4)
            plan.add(b_on(j, 0 if d > 0 else 1), needs=[by_one[j][0 if d > 0 else 1]], after=[layer[d]], cost=0.06, rank=2)

    a_sum, a_own = second(lambda j: (a_end, [ax_fin[j]], [layer[j]]), a2, ay1, ayf, yp, ym, rs_a, ry_a)
    b_sum, b_own = second(lambda j: (b_end, [by_fin[j]], [layer[0]]), b2, bx1, bxf, xp, xm, rs_b, rx_b)
    z_same, z_other, x_in = group(7), group(8), group(7)

    za_same, za_other, zb_same, zb_other = group(7), group(8), group(7), group(8)

    def z_out(buf, into, at, same, other):
        def run():
            sums = plus(buf[3], into[0], into[1], into[2])
            z3[0, :, :, at : at + 256] = sums[:, :, 0:256]
            z3[1, :, :, at : at + 256] = sums[:, :, 256:512]
            here = pl.ds(at, 256)
            for d in (4, 3, -3, 2, -2, 1, -1, 0):
                k = (d + NZ) % NZ
                send(z3.at[1 - c, za(d), :, here], r3.at[1, k, :, here], dict(dz=d, dc=1), rs_z, other)
                if d:
                    send(z3.at[c, za(d), :, here], r3.at[0, k, :, here], dict(dz=d), rs_z, same)

        return run

    def c_out_x():
        sums_c = plus(*(ry[slot[q]] for q in (1, -1, 2)), c2[slot[0]])
        c3[0] = sums_c[:, :, 0:256]
        c3[1] = sums_c[:, :, 256:512]
        for d in (2, 1, -1, 0):
            k = (d + NX) % NX
            send(c3.at[1 - c, xa(d)], rx.at[1, k], dict(dx=d, dc=1), rs_z, x_in)
            if d:
                send(c3.at[c, xa(d)], rx.at[0, k], dict(dx=d), rs_z, x_in)

    def out_z(at):
        def run():
            cols = slice(at, at + 256)
            total = res_s[c, :, cols].astype(F32) + z3[c, z, :, cols].astype(F32)
            for d in range(1, NZ):
                total = total + r3[0, d, :, cols].astype(F32)
            out[c, :, cols] = total.astype(BF16)
            total = res_in[:, cols].astype(F32)
            for d in range(NZ):
                total = total + r3[1, d, :, cols].astype(F32)
            out[1 - c, :, cols] = total.astype(BF16)

        return run

    def out_c():
        out[c, :, 512:768] = plus(res_s[c, :, 512:768], c3[c, x], rx[0, 1], rx[0, 2], rx[0, 3])
        out[1 - c, :, 512:768] = plus(res_in[:, 512:768], rx[1, 0], rx[1, 1], rx[1, 2], rx[1, 3])

    def out_c_same():
        total = res_s[c, :, 512:768].astype(F32)
        for k in range(NY):
            for i in range(NX):
                total = total + (c4[3, c, x] if k == 3 and i == 0 else rxy[0, k, i]).astype(F32)
        out[c, :, 512:768] = total.astype(BF16)

    def out_c_other():
        total = res_in[:, 512:768].astype(F32)
        for k in range(NY):
            for i in range(NX):
                total = total + rxy[1, k, i].astype(F32)
        out[1 - c, :, 512:768] = total.astype(BF16)

    a_sent = plan.add(z_out(a2, ry_a, 0, za_same, za_other), needs=[a_sum], after=[a_own], cost=0.12, rank=0)
    b_sent = plan.add(z_out(b2, rx_b, 256, zb_same, zb_other), needs=[b_sum], after=[b_own], cost=0.12, rank=0)
    if V3R:
        plan.add(out_c_same, needs=[resid_in, xy_same], after=c_ends, cost=0.1)
        plan.add(out_c_other, needs=[resid_in, xy_other], after=c_ends, cost=0.1)
    else:
        x_sent = plan.add(c_out_x, needs=[cy_in], after=c_ends, cost=0.1, rank=0)
        plan.add(out_c, needs=[resid_in, x_in], after=[x_sent], cost=0.1)
    plan.add(out_z(0), needs=[resid_in, za_same, za_other], after=[a_sent], cost=0.1)
    plan.add(out_z(256), needs=[resid_in, zb_same, zb_other], after=[b_sent], cost=0.1)
    plan.run()
    with scope("drain"):
        for sent in families:
            all_of(sent).wait_send()
    assert len(families) <= N_SEND and len(groups) <= N_RECV, (len(families), len(groups))
    assert max(g.tiles for g in families + groups) <= N_TILES


def exchange(part, tokens, mid_gain, ids, weights, blend, eg, eu, ed, dg, du, dd):
    vm = pl.BlockSpec(memory_space=VMEM)
    hbm = pl.BlockSpec(memory_space=pl.ANY)
    return pl.pallas_call(
        exchange_kernel,
        name="exchange",
        out_shape=jax.ShapeDtypeStruct((2, ROWS, D // 2), BF16),
        in_specs=[hbm] * 12,
        out_specs=vm,
        scratch_shapes=[
            VMEM((2, ROWS, D), BF16), VMEM((2, ROWS, D), BF16), VMEM((D // 128, 128), F32),
            VMEM(ids.shape, ids.dtype), VMEM(weights.shape, F32), VMEM((D,), BF16),
            VMEM((NX, NY, NZ, ROWS, WIDE), BF16),
            VMEM((NX, NY, NZ, ROWS, D), BF16),
            VMEM((2, 512, D), BF16),
            VMEM((2, 256, D), BF16),
            VMEM((2, ROWS, 128), F32),
            VMEM((4, 2, 256, 512), F32),
            VMEM((ROWS, D), BF16), VMEM((2, ROWS, D // 2), BF16), VMEM((ROWS, D // 2), BF16),
            VMEM((4, 2, 4, ROWS, W), BF16), VMEM((4, 2, NZ, ROWS, W), BF16),
            VMEM((2, 4, ROWS, W), BF16), VMEM((2, NZ, ROWS, W), BF16),
            VMEM((2, 4, ROWS, W), BF16), VMEM((2, NZ, ROWS, W), BF16),
            VMEM((4, 2, 4, ROWS, W), BF16), VMEM((4, 2, NZ, ROWS, W), BF16),
            VMEM((4, NZ, ROWS, W), BF16), VMEM((4, NZ, ROWS, W), BF16),
            VMEM((2, NZ, ROWS, W), BF16), VMEM((2, NZ, ROWS, W), BF16),
            VMEM((2, 4, 4, NX, ROWS, W), BF16), VMEM((4, NX, ROWS, W), BF16),
            VMEM((4, NX, ROWS, W), BF16), VMEM((2, NX, ROWS, W // 2), BF16),
            VMEM((2, NX, ROWS, W // 2), BF16),
            VMEM((3, NZ, ROWS, W), BF16), VMEM((3, NZ, ROWS, W), BF16),
            VMEM((2, NY, NX, ROWS, W // 2), BF16), VMEM((4, 2, NX, ROWS, W // 2), BF16),
            VMEM((4, 4, NX, ROWS, W), BF16), VMEM((2, 2, 4, NX, ROWS, W), BF16),
            VMEM((N_TILES, ROWS, 128), BF16),
            pltpu.SemaphoreType.DMA((N_SEND,)),
            pltpu.SemaphoreType.DMA((N_RECV,)),
            pltpu.SemaphoreType.DMA((22,)),
        ],
        compiler_params=pltpu.CompilerParams(collective_id=0, has_side_effects=True),
    )(part, tokens, mid_gain, ids, weights, blend, eg, eu, ed, dg, du, dd)


def shards(
    tokens, prior_state, first_gain, query_weight, key_weight, value_weight, decay_down, decay_up,
    decay_base, rate_down, rate_up, rate_base, head_gain, out_weight, mid_gain, route_ids,
    route_weights, expert_gate, expert_up, expert_down, dense_gate, dense_up, dense_down,
    blend_vector,
):
    part, new_state = mixer(
        tokens, prior_state, first_gain, query_weight, key_weight, value_weight, decay_down,
        decay_up, decay_base, rate_down, rate_up, rate_base, head_gain, out_weight,
    )
    mixed = exchange(
        part, tokens.reshape(2, ROWS, D), mid_gain.reshape(-1, 128), route_ids.T, route_weights.T,
        blend_vector, jnp.swapaxes(expert_gate, 1, 2),
        jnp.swapaxes(expert_up, 1, 2), expert_down, dense_gate.T, dense_up.T, dense_down,
    )
    return (mixed.reshape(2 * ROWS, D // 2), new_state)


def solution(mesh):
    split = Mesh(mesh.devices.reshape(NZ, NY, NX, mesh.shape["tp"]), EP_TP)
    in_specs = (
        P(EP, None),
        P(EP, "tp", None, None),
        P(),
        P(None, "tp"),
        P(None, "tp"),
        P(None, "tp"),
        P(),
        P(None, "tp"),
        P("tp"),
        P(),
        P(None, "tp"),
        P("tp"),
        P("tp"),
        P("tp", None),
        P(),
        P(EP, None),
        P(EP, None),
        P(EP, None, "tp"),
        P(EP, None, "tp"),
        P(EP, "tp", None),
        P(None, EP_TP),
        P(None, EP_TP),
        P(EP_TP, None),
        P(),
    )
    out_specs = (P(EP, "tp"), P(EP, "tp", None, None))
    return jax.shard_map(
        shards, mesh=split, in_specs=in_specs, out_specs=out_specs, check_vma=False
    )
```

time: 77 us -> 67.1 us (0.87)
  Pallas kernels: 74.7 us -> 64.9 us
    pallas_call x1, Pallas kernels: 66.5 us -> 57.5 us  [exchange(): pl.pallas_call(exchange_kernel, name='exchange', out_shape=jax.ShapeDtype...]
    pallas_call x1, Pallas kernels: 8.28 us -> 7.39 us  [mixer(): pl.pallas_call(mixer_kernel, name='mixer', out_shape=(jax.ShapeDtypeStruc...]
where the time goes in v3:
time: 67.1 us; the launch traced here: 66.9 us
  Pallas kernels  64.9 us (97%)
  local copies, waits for them, and re-layouts  1.35 us (2%)
    pallas_call x1, Pallas kernels, exchange(): pl.pallas_call(exchange_kernel, name='exchange', out_shape=jax.ShapeDtype...  57.5 us
    pallas_call x1, Pallas kernels, mixer(): pl.pallas_call(mixer_kernel, name='mixer', out_shape=(jax.ShapeDtypeStruc...  7.39 us
    unnamed x1, local copies, waits for them, and re-layouts  1.35 us

profile of v3, /device:TPU:1, one launch (start us, length us, event | category | flops | bytes accessed | tf_op | source)
XLA Modules:
  0.0 66.9 jit_solution(4774303946287441508)
XLA Ops:
  0.6 7.4 %mixer.1 = (bf16[2,8,1536]{2,1,0:T(8,128)(2,1)}, f32[16,6,64,64]{3,2,1,0:T(8,128)}) custom-call(bf16[16,1536]{1,0:T(8,128)(2,1)} %tok_h.1, f32[12,128]{1,0:T(8,128)} %bitcast.23, bf16[1536,384]{1,0:T(8,128)(2,1)} %wq_h.1, bf16[1536,384]{1,0:T(8,128)(2,1)} %wk_h.1, bf16[1536,384]{1,0:T(8,128)(2,1)} %wv_h.1, bf16[96,1536]{1,0:T(8,128)(2,1)} %bitcast.17, ...), custom_call_target="tpu_custom_call" | custom-call | tf_op jit(solution)/shard_map/mixer/pallas_call | solution.py:173
  8.0 57.5 %exchange.1 = bf16[2,8,768]{2,1,0:T(8,128)(2,1)} custom-call(bf16[2,8,1536]{2,1,0:T(8,128)(2,1)} %get-tuple-element.4.part_h, bf16[2,8,1536]{2,1,0:T(8,128)(2,1)} %bitcast.19, f32[12,128]{1,0:T(8,128)} %bitcast.24, s32[6,16]{1,0:T(8,128)} %bitcast.25, f32[6,16]{1,0:T(8,128)} %bitcast.26, bf16[1536]{0:T(1024)(128)(2,1)} %blend_h.1, ...), custom_call_target="tpu_custom_call" | custom-call | tf_op jit(solution)/shard_map/exchange/pallas_call | solution.py:903
  65.6 1.3 %copy.27 = bf16[16,768]{1,0:T(8,128)(2,1)} copy(bf16[16,768]{1,0:T(8,128)(2,1)} %bitcast.20) | data formatting | bytes 49152
